TPU v7x, 512 devices: a whole 4x8x8 slice. The times are simulated.
512 devices in a mesh: sp: 32 (over z, x), tp: 16 (over y, core).
Axes of the slice: x: 4, y: 8, z: 8, core: 2. Of those that a mesh axis runs over, the one named last changes fastest.
Arguments:
- tokens: bfloat16 [65536, 4096], P(('sp', 'tp')), may hold values from -6 to 6
- lock_projector: bfloat16 [4096, 1024], P(None, 'tp'), may hold values from -0.01171875 to 0.01171875
- value_weight: bfloat16 [4096, 2048], P(None, 'tp'), may hold values from -0.0234375 to 0.0234375
- decay_weight: bfloat16 [4096, 1024], P(None, 'tp'), may hold values from -0.09375 to 0.09375
- decay_offset: float32 [1024], P('tp'), may hold values from -3.5 to 0
- fresh_question: bfloat16 [16, 64], P('tp'), may hold values from -6 to 6
Outputs:
- state_cache: bfloat16 [16, 64, 128], P('tp', 'sp')
- first_read: bfloat16 [16, 128], P('tp')
All inputs are finite; a program needn't handle non-finite values.
Results may differ from a plain program's by a relative error of at most 0.0034.
Values may be sent and summed in bfloat16 or wider, within the bound.
A program may use at most 64 MiB of HBM per device.

v0:
```python
import math

import jax
import jax.numpy as jnp
from jax import lax
from jax.sharding import PartitionSpec as P

CUE_WIDTH = 64
DV = 128


decay_tau = 16.0


def sent_to_all(x, axis):
    copies = jnp.broadcast_to(x, (lax.axis_size(axis), *x.shape))
    return lax.all_to_all(copies, axis, split_axis=0, concat_axis=0, tiled=True)


def folded_in_pairs(pieces, combine):
    while len(jax.tree.leaves(pieces)[0]) > 1:
        pieces = jax.vmap(combine)(*(pieces[side::2] for side in (0, 1)))
    return pieces[0]


def entering(x, axis, combine, identity):
    count, index = (lax.axis_size(axis), lax.axis_index(axis))
    passed = jnp.arange(count) > index

    def kept(part, zero, own):
        part = jnp.where(
            passed.reshape(-1, *(1 for _ in own.shape)), part, jnp.asarray(zero, own.dtype)
        )
        return part[::-1]

    pieces = sent_to_all(x, axis)
    return folded_in_pairs(kept(pieces, identity, x), combine)


def cut_along(x, dim, count):
    dims = x.shape
    pieces = x.reshape(*dims[:dim], count, dims[dim] // count, *dims[dim + 1 :])
    return jnp.moveaxis(pieces, dim, 0)


def sent_and_summed(x, axis, dim):
    pieces = cut_along(x, dim, lax.axis_size(axis))
    arrived = lax.all_to_all(pieces, axis, split_axis=0, concat_axis=0, tiled=True)
    return arrived.sum(axis=0)


def over_copies(x, axis):
    return sent_to_all(x, axis).sum(axis=0)


def add_logs(earlier, later_sum):
    return earlier + later_sum


def per_device(tokens, lock_projector, value_weight, decay_weight, decay_offset, fresh_question):
    key_cols = lock_projector.shape[1]
    value_cols = value_weight.shape[1]
    local_heads = key_cols // CUE_WIDTH
    combined = jnp.concatenate([lock_projector, value_weight, decay_weight], axis=1)
    projected = jnp.dot(
        lax.all_gather(tokens, "tp", axis=0, tiled=True),
        combined,
        preferred_element_type=jnp.float32,
    )
    span_rows = projected.shape[0]
    lock_vectors = projected[:, :key_cols].astype(jnp.bfloat16)
    value_rows = projected[:, key_cols : key_cols + value_cols].astype(jnp.bfloat16)
    decay_pre = projected[:, key_cols + value_cols :]
    length = span_rows * lax.axis_size("sp")
    log_decay = jax.nn.log_sigmoid(decay_pre + decay_offset[None, :] + math.log(length)) / decay_tau
    segment_overall = jnp.sum(log_decay, axis=0)
    later_total = entering(segment_overall, "sp", add_logs, jnp.zeros_like(segment_overall))
    after = (segment_overall + later_total)[None, :] - jnp.cumsum(log_decay, axis=0)
    weighted = (lock_vectors.astype(jnp.float32) * jnp.exp(after)).astype(jnp.bfloat16)
    lookup_probes = weighted.reshape(span_rows, local_heads, CUE_WIDTH)
    stored_contents = value_rows.reshape(span_rows, local_heads, DV)
    summands_list = jnp.einsum(
        "nyl,nyp->ylp", lookup_probes, stored_contents, preferred_element_type=jnp.float32
    )
    key_scale = CUE_WIDTH ** (-0.5)
    question_widened = fresh_question.astype(jnp.float32)
    row_span = CUE_WIDTH // lax.axis_size("sp")
    row_start = lax.axis_index("sp") * row_span
    segment_lines = sent_and_summed(summands_list, "sp", 1)
    query_rows = lax.dynamic_slice_in_dim(question_widened, row_start, row_span, 1)
    partial_read = key_scale * jnp.einsum(
        "qw,qwi->qi", query_rows, segment_lines, precision=lax.Precision.HIGHEST
    )
    attended_blend = over_copies(partial_read, "sp")
    state_cache = segment_lines.astype(jnp.bfloat16)
    first_read = attended_blend * lax.rsqrt(
        jnp.mean(attended_blend * attended_blend, axis=-1, keepdims=True) + 1.0
    )
    return (state_cache, first_read.astype(jnp.bfloat16))


def solution(mesh):
    in_specs = (
        P(("sp", "tp"), None),
        P(None, "tp"),
        P(None, "tp"),
        P(None, "tp"),
        P("tp"),
        P("tp", None),
    )
    out_specs = (P("tp", "sp", None), P("tp", None))
    return jax.shard_map(
        per_device, mesh=mesh, in_specs=in_specs, out_specs=out_specs, check_vma=False
    )
```

profile of v0, /device:TPU:1, one launch (start us, length us, event | category | flops | bytes accessed | tf_op | source)
XLA Modules:
  0.0 199.8 jit_solution(17577149090542272059)
XLA Ops:
  7.2 0.0 copy-start
  7.2 0.0 all-gather.2.cloned.1.call-start
  7.2 0.7 all-gather.2.cloned.1.call-update
  7.9 1.5 copy.32
  9.4 1.5 copy.33
  11.0 0.0 copy-start.1
  11.0 102.7 %all-gather.2.cloned.1.call-done = bf16[2048,4096]{1,0:T(8,128)(2,1)} async-done(((bf16[128,4096]{1,0:T(8,128)(2,1)}), bf16[2048,4096]{1,0:T(8,128)(2,1)}) %all-gather.2.cloned.1.call-update) | async-done | bytes 16777232 | tf_op jit(solution)/shard_map/all_gather | solution.py:66
  113.7 13.1 %fusion.21 = (bf16[2048,256]{0,1:T(8,128)(2,1)S(1)}, f32[2048,256]{0,1:T(8,128)}) fusion(bf16[2048,4096]{1,0:T(8,128)(2,1)} %all-gather.2.cloned.1.call-done, bf16[4096,64]{1,0:T(8,128)(2,1)S(1)} %copy.33, bf16[4096,128]{1,0:T(8,128)(2,1)} %param.8, bf16[4096,64]{1,0:T(8,128)(2,1)S(1)} %copy.32), kind=kOutput, calls=%fused_computation.36 | convolution fusion | flops 4301783040 | bytes 22020096 | tf_op jit(solution)/shard_map/dot_general | solution.py:65
  126.8 0.0 copy-done.1
  126.8 1.6 fusion.20
  128.4 0.6 broadcast_in_dim.23
  129.0 9.9 %all-to-all-start = ((f32[32,1,64]{2,1,0:T(1,128)}), f32[32,1,64]{2,1,0:T(1,128)S(1)}, u32[]{:S(2)}, u32[]{:S(2)}) async-start(f32[32,1,64]{2,1,0:T(1,128)} %broadcast_in_dim.23), calls=%async_computation | async-start | bytes 32768 | tf_op jit(solution)/shard_map/all_to_all | solution.py:17
  138.9 0.1 copy.43
  139.0 18.1 %reduce-window.6 = f32[64,16,128]{2,1,0:T(8,128)S(1)} reduce-window(f32[64,16,128]{2,1,0:T(8,128)S(1)} %bitcast.60, f32[]{:T(128)} %constant.12.clone.1), window={size=1x1x128 pad=0_0x0_0x127_0}, to_apply=%region_1.2 | reduce-window | flops 16646144 | bytes 1048580 | tf_op jit(solution)/shard_map/reduce-window
  157.1 0.2 slice.74
  157.3 0.4 copy.41
  157.8 0.2 reduce-window.9
  158.0 0.2 broadcast_add_fusion
  158.2 0.0 all-to-all-done
  158.2 0.1 broadcast_select_fusion
  158.5 0.3 fusion.14
  158.7 0.2 reshape.90
  158.9 0.3 convolution_bitcast_fusion.1
  159.2 0.6 copy.38
  159.9 9.2 %all-to-all-start.1 = ((f32[32,1,2,128]{3,2,1,0:T(2,128)}), f32[32,1,2,128]{3,2,1,0:T(2,128)S(1)}, u32[]{:S(2)}, u32[]{:S(2)}) async-start(f32[32,1,2,128]{3,2,1,0:T(2,128)} %copy.38), calls=%async_computation.1 | async-start | bytes 65536 | tf_op jit(solution)/shard_map/all_to_all | solution.py:48
  169.1 8.7 %all-to-all-done.1 = f32[32,1,2,128]{3,2,1,0:T(2,128)S(1)} async-done(((f32[32,1,2,128]{3,2,1,0:T(2,128)}), f32[32,1,2,128]{3,2,1,0:T(2,128)S(1)}, u32[]{:S(2)}, u32[]{:S(2)}) %all-to-all-start.1) | async-done | bytes 32800 | tf_op jit(solution)/shard_map/all_to_all | solution.py:48
  177.8 0.0 copy-done
  177.8 0.2 fusion.5
  178.0 0.6 broadcast_in_dim.25
  178.6 3.9 %all-to-all-start.2 = ((f32[32,1,128]{2,1,0:T(1,128)}), f32[32,1,128]{2,1,0:T(1,128)S(1)}, u32[]{:S(2)}, u32[]{:S(2)}) async-start(f32[32,1,128]{2,1,0:T(1,128)} %broadcast_in_dim.25), calls=%async_computation.2 | async-start | bytes 32768 | tf_op jit(solution)/shard_map/all_to_all | solution.py:17
  182.5 0.5 convert_bitcast_fusion.1
  183.0 8.1 %all-to-all-done.2 = f32[32,1,128]{2,1,0:T(1,128)S(1)} async-done(((f32[32,1,128]{2,1,0:T(1,128)}), f32[32,1,128]{2,1,0:T(1,128)S(1)}, u32[]{:S(2)}, u32[]{:S(2)}) %all-to-all-start.2) | async-done | bytes 16416 | tf_op jit(solution)/shard_map/all_to_all | solution.py:17
  191.1 0.6 multiply_reduce_fusion
  192.4 0.5 convert_bitcast_fusion
  (18 shorter events, 0.3 us)
Async XLA Ops:
  7.2 170.7 %copy-start = (bf16[1,64]{1,0:T(2,128)(2,1)S(1)}, bf16[1,64]{1,0:T(2,128)(2,1)}, u32[]{:S(2)}) copy-start(bf16[1,64]{1,0:T(2,128)(2,1)} %param.11) | copy-start | bytes 388
  7.2 106.5 %all-gather.2.cloned.1.call-start = ((), (), s32[]{:S(2)}) async-start(), calls=%async_computation.3 | async-start | bytes 17825792 | tf_op jit(solution)/shard_map/all_gather | solution.py:66
  11.0 115.8 %copy-start.1 = (f32[64]{0:T(128)S(1)}, f32[64]{0:T(128)}, u32[]{:S(2)}) copy-start(f32[64]{0:T(128)} %param.10) | copy-start | bytes 772
  129.0 29.2 %all-to-all-start = ((f32[32,1,64]{2,1,0:T(1,128)}), f32[32,1,64]{2,1,0:T(1,128)S(1)}, u32[]{:S(2)}, u32[]{:S(2)}) async-start(f32[32,1,64]{2,1,0:T(1,128)} %broadcast_in_dim.23), calls=%async_computation | async-start | bytes 32768 | tf_op jit(solution)/shard_map/all_to_all | solution.py:17
  159.9 17.9 %all-to-all-start.1 = ((f32[32,1,2,128]{3,2,1,0:T(2,128)}), f32[32,1,2,128]{3,2,1,0:T(2,128)S(1)}, u32[]{:S(2)}, u32[]{:S(2)}) async-start(f32[32,1,2,128]{3,2,1,0:T(2,128)} %copy.38), calls=%async_computation.1 | async-start | bytes 65536 | tf_op jit(solution)/shard_map/all_to_all | solution.py:48
  178.6 12.5 %all-to-all-start.2 = ((f32[32,1,128]{2,1,0:T(1,128)}), f32[32,1,128]{2,1,0:T(1,128)S(1)}, u32[]{:S(2)}, u32[]{:S(2)}) async-start(f32[32,1,128]{2,1,0:T(1,128)} %broadcast_in_dim.25), calls=%async_computation.2 | async-start | bytes 32768 | tf_op jit(solution)/shard_map/all_to_all | solution.py:17
Sparse Core Ops, SparseCore 0:
  10.1 103.5 all-gather.1
where the time goes:
time: 201 us; the launch traced here: 200 us
  waiting for transfers between devices  120 us (60%)
  starting transfers between devices  23 us (11%)
  other arithmetic  22.2 us (11%)
  between operations  14.9 us (7%)
  matrix products  13.6 us (7%)
  local copies, waits for them, and re-layouts  6 us (3%)
    all_gather x1, waiting for transfers between devices, per_device(): lax.all_gather(tokens, 'tp', axis=0, tiled=True)  103 us
    another operation x3, other arithmetic  18.5 us
    all_to_all x2, starting transfers between devices, sent_to_all(): return lax.all_to_all(copies, axis, split_axis=0, concat_axis=0, tiled=True)  13.8 us
    dot_general x1, matrix products, per_device(): jnp.dot(lax.all_gather(tokens, 'tp', axis=0, tiled=True), combined, prefe...  13.1 us
    all_to_all x1, starting transfers between devices, sent_and_summed(): lax.all_to_all(pieces, axis, split_axis=0, concat_axis=0, tiled=True)  9.22 us
    all_to_all x1, waiting for transfers between devices, sent_and_summed(): lax.all_to_all(pieces, axis, split_axis=0, concat_axis=0, tiled=True)  8.7 us
    all_to_all x2, waiting for transfers between devices, sent_to_all(): return lax.all_to_all(copies, axis, split_axis=0, concat_axis=0, tiled=True)  8.11 us
  transfers between devices with their start and end apart: 4, of which 3 were waited for; matrix products, arithmetic and copies ran while one was open for 11% of the time, Pallas kernels for 0%

commit v1 on v0

v1 whole, which is shorter than its diff:
```python
import math

import jax
import jax.numpy as jnp
from jax import lax
from jax.experimental import pallas as pl
from jax.experimental.pallas import tpu as pltpu
from jax.sharding import PartitionSpec as P

F32 = jnp.float32
BF16 = jnp.bfloat16
MESH = pl.DeviceIdType.MESH
NX, NY, NZ = 4, 8, 8
NSP = NX * NZ
D = 4096
CUE = 64
DV = 128
ROWS = 128
CHIP = 2 * ROWS
SLICE = D // NZ
HALF = SLICE // 2
TAU = 16.0
LN_LENGTH = math.log(65536)


def log_sigmoid(t):
    u = jnp.exp(-jnp.abs(t))
    s = u / (u + 2.0)
    s2 = s * s
    series = jnp.full_like(s, 1.0 / 17.0)
    for odd in (15, 13, 11, 9, 7, 5, 3, 1):
        series = series * s2 + 1.0 / odd
    return jnp.minimum(t, 0.0) - 2.0 * s * series


def kernel(
    tok_hbm, lock_hbm, val_hbm, dec_hbm, off_ref, q_ref,
    state_out, read_out,
    tok, w, wsrc, lock_v, dec_v, offsrc, offs, acc, after, kk, weighted,
    tot, t1, t2, st, s1, s2src, s2,
    load_sem, y_send, y_recv, o_send, o_recv, z_send, z_recv, x_send, x_recv, d_send, d_recv,
    t1_send, t1_recv, t2_send, t2_recv, s1_send, s1_recv, s2_send, s2_recv,
):
    sp = lax.axis_index("sp")
    tp = lax.axis_index("tp")
    z = sp // NX
    x = sp % NX
    y = tp // 2
    c = tp % 2

    def dev(x_, y_, z_, c_=None):
        return {"sp": z_ * NX + x_, "tp": y_ * 2 + (c if c_ is None else c_)}

    o = (x, 4 + (4 - x) % 4)
    up = [(y + o[s]) % NY for s in range(2)]
    down = [(y - o[s] + NY) % NY for s in range(2)]
    xr, xl = (x + 1) % NX, (x + 3) % NX
    zr, zl = (z + 1) % NZ, (z + 7) % NZ
    x2 = (x + 2) % NX
    mine = c * ROWS
    other = (1 - c) * ROWS

    zrow = pl.multiple_of(z * SLICE, SLICE)
    loads = [
        pltpu.make_async_copy(lock_hbm.at[pl.ds(zrow, SLICE)], lock_v, load_sem.at[0]),
        pltpu.make_async_copy(dec_hbm.at[pl.ds(zrow, SLICE)], dec_v, load_sem.at[1]),
        pltpu.make_async_copy(val_hbm.at[pl.ds(zrow, SLICE)], wsrc.at[1], load_sem.at[2]),
        pltpu.make_async_copy(tok_hbm, tok.at[x, pl.ds(pl.multiple_of(mine, ROWS), ROWS)], load_sem.at[3]),
    ]
    for load in loads:
        load.start()

    barrier = pltpu.get_barrier_semaphore()

    def greet(device):
        pl.semaphore_signal(barrier, inc=1, device_id=device, device_id_type=MESH)

    greet(dev(x, y, z, 1 - c))
    greet(dev(x, up[1], z))
    greet(dev(x, down[1], z))

    def t1_peer(s, dy):
        yy = (y + dy) % NY
        d = (up[s] - yy + NY) % NY
        r = d // 4
        return (d + r * (8 - 2 * d)) % NX, yy, r

    def greet_row(dy, carry):
        for s in range(2):
            xx, yy, _ = t1_peer(s, dy)
            greet(dev(xx, yy, z))
        return carry

    lax.fori_loop(1, NY, greet_row, 0)

    def greet_sp(i, carry):
        greet({"sp": (sp + i) % NSP, "tp": tp})
        return carry

    lax.fori_loop(1, NSP, greet_sp, 0)

    lane = lax.broadcasted_iota(jnp.int32, (1, 128), 1)
    low = lane < CUE
    offsrc[...] = jnp.broadcast_to(jnp.concatenate([off_ref[...], off_ref[...]], axis=1), offsrc.shape)
    loads[0].wait()
    loads[1].wait()
    wsrc[0] = jnp.concatenate([lock_v[...], dec_v[...]], axis=1)
    loads[2].wait()
    loads[3].wait()

    pl.semaphore_wait(barrier, 3 + 2 * (NY - 1) + NSP - 1)

    def remote(src, dst, send, recv, device):
        return pltpu.make_async_remote_copy(
            src_ref=src, dst_ref=dst, send_sem=send, recv_sem=recv, device_id=device, device_id_type=MESH
        )

    def y_copy(s, k):
        t, j = k // 2, k % 2
        rows = pl.ds(pl.multiple_of(z * SLICE + j * HALF, HALF), HALF)
        return remote(
            wsrc.at[t, pl.ds(j * HALF, HALF)],
            w.at[t, rows, pl.ds(s * 128, 128)],
            y_send.at[s, k], y_recv.at[s, k], dev(x, down[s], z),
        )

    def o_copy(s):
        return remote(offsrc, offs.at[s], o_send.at[s], o_recv.at[s], dev(x, down[s], z))

    for k in range(4):
        y_copy(1, k).start()

        @pl.when(x != 0)
        def _():
            y_copy(0, k).start()

        if k == 0:
            o_copy(1).start()

            @pl.when(x != 0)
            def _():
                o_copy(0).start()

    @pl.when(x == 0)
    def _():
        rows = pl.ds(zrow, SLICE)
        for t in range(2):
            w[t, rows, 0:128] = wsrc[t]
        offs[0] = offsrc[...]

    def x_block(direction, seg):
        half = direction if seg != 1 else 1 - direction
        back = 2 if seg == 2 else 1
        return half, back

    def x_copy(direction, seg):
        half, back = x_block(direction, seg)
        owner = x if back == 1 else (xl if direction == 0 else xr)
        ref = tok.at[owner, pl.ds(pl.multiple_of(mine + half * 64, 64), 64)]
        return remote(ref, ref, x_send.at[direction, seg], x_recv.at[direction, seg],
                      dev(xr if direction == 0 else xl, y, z))

    for seg in range(2):
        for direction in range(2):
            x_copy(direction, seg).start()

    def d_rows(n):
        if n == 0:
            return x, 0, ROWS
        direction, seg = (n - 1) % 2, (n - 1) // 2
        half, back = x_block(direction, seg)
        owner = x2 if back == 2 else (xl if direction == 0 else xr)
        return owner, half * 64, 64

    def d_copy(n):
        owner, start, size = d_rows(n)
        ref = tok.at[owner, pl.ds(pl.multiple_of(mine + start, 64), size)]
        return remote(ref, ref, d_send.at[n], d_recv.at[n], dev(x, y, z, 1 - c))

    d_copy(0).start()

    def z_ref(direction, k, d, hop):
        t, j = k // 2, k % 2
        owner = (z - d + NZ) % NZ if direction == 0 else (z + d) % NZ
        start, size = owner * SLICE + j * HALF, HALF
        if hop == 3:
            start, size = start + direction * (HALF // 2), HALF // 2
        return w.at[t, pl.ds(pl.multiple_of(start, HALF // 2), size)]

    def z_copy(direction, k, d):
        ref = z_ref(direction, k, d, d)
        return remote(ref, ref, z_send.at[direction, k, d], z_recv.at[direction, k, d],
                      dev(x, y, zr if direction == 0 else zl))

    def z_wait(direction, k, d):
        ref = z_ref(direction, k, d + 1, d)
        remote(ref, ref, z_send.at[direction, k, d], z_recv.at[direction, k, d], dev(x, y, zr)).wait_recv()

    def own(k):
        y_copy(1, k).wait_recv()

        @pl.when(x != 0)
        def _():
            y_copy(0, k).wait_recv()

        for direction in range(2):
            z_copy(direction, k, 0).start()

    def hop(k, d):
        for direction in range(2):
            z_wait(direction, k, d - 1)
            z_copy(direction, k, d).start()

    def last(k):
        for direction in range(2):
            z_wait(direction, k, 3)

    acc[...] = jnp.zeros_like(acc)

    def project(t, block, piece):
        cols = pl.ds(pl.multiple_of(piece * SLICE, SLICE), SLICE)
        out = pl.ds(pl.multiple_of(block * CHIP, CHIP), CHIP)
        acc[t, out] += jnp.dot(tok[block, :, cols], w[t, cols], preferred_element_type=F32)

    def project_blocks(t, piece, first, count):
        def body(i, carry):
            project(t, (x + first + i) % NX, piece)
            return carry

        lax.fori_loop(0, count, body, 0)

    def project_pieces(t, block, start, count):
        def body(i, carry):
            project(t, block, (z + start + i) % NZ)
            return carry

        lax.fori_loop(0, count, body, 0)

    own(0)
    own(1)
    d_copy(0).wait_recv()
    hop(0, 1)
    hop(1, 1)
    project_pieces(0, x, NZ - 1, 3)
    for direction in range(2):
        x_copy(direction, 0).wait_recv()
        x_copy(direction, 2).start()
        d_copy(1 + direction).start()
    hop(0, 2)
    hop(1, 2)
    project_pieces(0, x, 2, 1)
    project_pieces(0, x, NZ - 2, 1)
    hop(0, 3)
    hop(1, 3)
    own(2)
    own(3)
    project_pieces(0, x, 3, 1)
    project_pieces(0, x, NZ - 3, 1)
    for direction in range(2):
        x_copy(direction, 1).wait_recv()
        d_copy(3 + direction).start()
    last(0)
    last(1)
    project_pieces(0, x, 4, 1)
    hop(2, 1)
    for n in range(1, 5):
        d_copy(n).wait_recv()
    project_pieces(0, xr, 0, NZ)
    hop(3, 1)
    project_pieces(0, xl, 0, NZ)
    hop(2, 2)
    for direction in range(2):
        x_copy(direction, 2).wait_recv()
        d_copy(5 + direction).start()
    for n in range(5, 7):
        d_copy(n).wait_recv()
    project_pieces(0, x2, 0, NZ)
    hop(3, 2)

    o_copy(1).wait_recv()

    @pl.when(x != 0)
    def _():
        o_copy(0).wait_recv()

    offset = jnp.where(low, offs[0, 0:1], offs[1, 0:1])
    later_rows = (
        lax.broadcasted_iota(jnp.int32, (CHIP, CHIP), 1) > lax.broadcasted_iota(jnp.int32, (CHIP, CHIP), 0)
    ).astype(BF16)

    def decay(b, carry):
        rows = pl.ds(pl.multiple_of(b * CHIP, CHIP), CHIP)
        first, second = acc[0, rows, 0:128], acc[0, rows, 128:256]
        kk[rows] = jnp.where(low, first, pltpu.roll(second, CUE, 1)).astype(BF16)
        pre = jnp.where(low, pltpu.roll(first, CUE, 1), second)
        log_decay = log_sigmoid(pre + offset + LN_LENGTH) * (1.0 / TAU)
        high = log_decay.astype(BF16)
        rest = log_decay - high.astype(F32)
        middle = rest.astype(BF16)
        small = (rest - middle.astype(F32)).astype(BF16)
        sums = jnp.dot(later_rows, jnp.concatenate([high, middle, small], axis=1), preferred_element_type=F32)
        local = sums[:, 256:384] + sums[:, 128:256] + sums[:, 0:128]
        after[rows] = local
        total = local[0:1] + log_decay[0:1]
        tot[0, b] = total
        tot[1, b] = pltpu.roll(total, CUE, 1)
        return carry

    lax.fori_loop(0, NX, decay, 0)

    def t1_copy(s, dy):
        xx, yy, r = t1_peer(s, dy)
        differs = (r + s) % 2
        return remote(tot.at[differs], t1.at[r, y], t1_send, t1_recv, dev(xx, yy, z))

    def t1_start(dy, carry):
        for s in range(2):
            t1_copy(s, dy).start()
        return carry

    lax.fori_loop(1, NY, t1_start, 0)
    for s in range(2):
        t1[s, y] = tot[0]

    for i in range(3):
        piece = (z + (0, 1, NZ - 1)[i]) % NZ
        project_blocks(1, piece, 0, NX)
    hop(2, 3)
    hop(3, 3)

    t1_bytes = t1.at[:, 0 : NY - 1]
    remote(t1_bytes, t1_bytes, t1_send, t1_recv, dev(x, y, z, 1 - c)).wait_recv()
    blocks = jnp.where(low[None, None], t1[0], t1[1])
    per_x = jnp.sum(blocks, axis=0)
    y_index = lax.broadcasted_iota(jnp.int32, blocks.shape, 0)
    later_y = jnp.sum(jnp.where(y_index > y, blocks, 0.0), axis=0)
    span = per_x[0] + per_x[1] + per_x[2] + per_x[3]
    t2[z] = span

    def t2_copy(i):
        return remote(t2.at[z], t2.at[z], t2_send, t2_recv, dev(x, y, (z + i) % NZ))

    def t2_start(i, carry):
        t2_copy(i).start()
        return carry

    lax.fori_loop(1, NZ, t2_start, 0)

    for i in range(2):
        piece = (z + (2, NZ - 2)[i]) % NZ
        project_blocks(1, piece, 0, NX)

    t2_bytes = t2.at[0 : NZ - 1]
    remote(t2_bytes, t2_bytes, t2_send, t2_recv, dev(x, y, z, 1 - c)).wait_recv()
    spans = t2[...]
    z_index = lax.broadcasted_iota(jnp.int32, spans.shape, 0)
    later = jnp.sum(jnp.where(z_index > z, spans, 0.0), axis=0)
    for b in range(NX - 1, -1, -1):
        rows = pl.ds(b * CHIP, CHIP)
        factor = jnp.exp(after[rows] + (later + later_y[b]))
        weighted[rows] = (kk[rows].astype(F32) * factor).astype(BF16)
        later = later + per_x[b]

    for i in range(2):
        piece = (z + (3, NZ - 3)[i]) % NZ
        project_blocks(1, piece, 0, NX)
    last(2)
    last(3)
    project_blocks(1, (z + 4) % NZ, 0, NX)

    state = lax.dot_general(
        weighted[...], acc[1].astype(BF16), (((0,), (0,)), ((), ())), preferred_element_type=F32
    )
    st[0] = state[0:CUE, 0:DV]
    st[1] = state[CUE:, DV:]

    def s1_copy(s):
        return remote(st.at[s], s1.at[s], s1_send.at[s], s1_recv.at[s], dev(x, up[s], z))

    s1_copy(1).start()

    @pl.when(x != 0)
    def _():
        s1_copy(0).start()

    @pl.when(x == 0)
    def _():
        s1[0] = state[0:CUE, 0:DV]

    eye = (
        lax.broadcasted_iota(jnp.int32, (CUE, CUE), 0) == lax.broadcasted_iota(jnp.int32, (CUE, CUE), 1)
    )
    question = jnp.sum(jnp.where(eye, q_ref[...].astype(F32), 0.0), axis=1, keepdims=True) * CUE ** -0.5

    s1_copy(1).wait_recv()

    @pl.when(x != 0)
    def _():
        s1_copy(0).wait_recv()

    summed = s1[0] + s1[1]
    term = jnp.sum(question * summed, axis=0, keepdims=True)
    s2src[:, 0:2] = summed.reshape(NSP, 2, DV)
    s2src[:, 2:4] = jnp.broadcast_to(term[None], (NSP, 2, DV))

    def s2_copy(i):
        peer = (sp + i) % NSP
        return remote(s2src.at[peer], s2.at[sp], s2_send, s2_recv, {"sp": peer, "tp": tp})

    def s2_start(i, carry):
        s2_copy(i).start()
        return carry

    lax.fori_loop(1, NSP, s2_start, 0)
    s2[sp] = s2src[sp]
    s2_bytes = s2.at[0 : NSP - 1]
    remote(s2_bytes, s2_bytes, s2_send, s2_recv, dev(x, y, z, 1 - c)).wait_recv()
    total = jnp.sum(s2[...], axis=0)
    state_out[...] = total[0:2].astype(BF16)
    heard = total[2:3]
    square = jnp.mean(heard * heard, axis=1, keepdims=True)
    read_out[...] = (heard * lax.rsqrt(square + 1.0)).astype(BF16)

    for k in range(4):
        y_copy(1, k).wait_send()

        @pl.when(x != 0)
        def _():
            y_copy(0, k).wait_send()

        for d in range(4):
            for direction in range(2):
                z_copy(direction, k, d).wait_send()
    o_copy(1).wait_send()
    s1_copy(1).wait_send()

    @pl.when(x != 0)
    def _():
        o_copy(0).wait_send()
        s1_copy(0).wait_send()

    for seg in range(3):
        for direction in range(2):
            x_copy(direction, seg).wait_send()
    for n in range(7):
        d_copy(n).wait_send()
    remote(t1_bytes, t1_bytes, t1_send, t1_recv, dev(x, y, z, 1 - c)).wait_send()
    remote(t2_bytes, t2_bytes, t2_send, t2_recv, dev(x, y, z, 1 - c)).wait_send()
    remote(s2_bytes, s2_bytes, s2_send, s2_recv, dev(x, y, z, 1 - c)).wait_send()


def per_device(tokens, lock_projector, value_weight, decay_weight, decay_offset, fresh_question):
    dma = pltpu.SemaphoreType.DMA
    anywhere = pl.BlockSpec(memory_space=pl.ANY)
    vmem = pl.BlockSpec(memory_space=pltpu.VMEM)
    state, read = pl.pallas_call(
        kernel,
        out_shape=(jax.ShapeDtypeStruct((2, DV), BF16), jax.ShapeDtypeStruct((1, DV), BF16)),
        in_specs=[anywhere] * 4 + [vmem] * 2,
        out_specs=(vmem, vmem),
        scratch_shapes=[
            pltpu.VMEM((NX, CHIP, D), BF16),
            pltpu.VMEM((2, D, 256), BF16),
            pltpu.VMEM((2, SLICE, 128), BF16),
            pltpu.VMEM((SLICE, CUE), BF16),
            pltpu.VMEM((SLICE, CUE), BF16),
            pltpu.VMEM((8, 128), F32),
            pltpu.VMEM((2, 8, 128), F32),
            pltpu.VMEM((2, NX * CHIP, 256), F32),
            pltpu.VMEM((NX * CHIP, 128), F32),
            pltpu.VMEM((NX * CHIP, 128), BF16),
            pltpu.VMEM((NX * CHIP, 128), BF16),
            pltpu.VMEM((2, NX, 1, 128), F32),
            pltpu.VMEM((2, NY, NX, 1, 128), F32),
            pltpu.VMEM((NZ, 1, 128), F32),
            pltpu.VMEM((2, CUE, DV), F32),
            pltpu.VMEM((2, CUE, DV), F32),
            pltpu.VMEM((NSP, 4, DV), F32),
            pltpu.VMEM((NSP, 4, DV), F32),
            dma((4,)),
            dma((2, 4)), dma((2, 4)),
            dma((2,)), dma((2,)),
            dma((2, 4, 4)), dma((2, 4, 4)),
            dma((2, 3)), dma((2, 3)),
            dma((7,)), dma((7,)),
            dma, dma,
            dma, dma,
            dma((2,)), dma((2,)),
            dma, dma,
        ],
        compiler_params=pltpu.CompilerParams(
            collective_id=0, has_side_effects=True, vmem_limit_bytes=48 * 1024 * 1024
        ),
    )(
        tokens, lock_projector, value_weight, decay_weight,
        decay_offset.reshape(1, CUE), fresh_question,
    )
    return state.reshape(1, 2, DV), read


def solution(mesh):
    in_specs = (
        P(("sp", "tp"), None),
        P(None, "tp"),
        P(None, "tp"),
        P(None, "tp"),
        P("tp"),
        P("tp", None),
    )
    out_specs = (P("tp", "sp", None), P("tp", None))
    return jax.shard_map(
        per_device, mesh=mesh, in_specs=in_specs, out_specs=out_specs, check_vma=False
    )
```

time: 201 us -> 96 us (0.48)
  waiting for transfers between devices: 120 us -> 0 us
  Pallas kernels: 0 us -> 89.6 us
  starting transfers between devices: 23 us -> 0 us
  other arithmetic: 22.2 us -> 0 us
  between operations: 14.9 us -> 0.71 us
  matrix products: 13.6 us -> 0 us
    all_gather x1 -> x0, waiting for transfers between devices: 103 us -> none  [per_device(): lax.all_gather(tokens, 'tp', axis=0, tiled=True)]
    pallas_call x0 -> x1, Pallas kernels: none -> 89.6 us  [per_device(): pl.pallas_call(kernel, out_shape=(jax.ShapeDtypeStruct((2, DV), BF16), ja...]
    all_to_all x3 -> x0, starting transfers between devices: 23 us -> none  [the longest x2 13.8 us: sent_to_all(): return lax.all_to_all(copies, axis, split_axis=0, concat_axis=0, tiled=True)]
    another operation x3 -> x0, other arithmetic: 18.5 us -> none
    all_to_all x3 -> x0, waiting for transfers between devices: 16.8 us -> none  [the longest x1 8.7 us: sent_and_summed(): lax.all_to_all(pieces, axis, split_axis=0, concat_axis=0, tiled=True)]
    dot_general x3 -> x0, matrix products: 13.6 us -> none  [the longest x1 13.1 us: per_device(): jnp.dot(lax.all_gather(tokens, 'tp', axis=0, tiled=True), combined, prefe...]
    reduce_sum x4 -> x0, other arithmetic: 2.24 us -> none  [the longest x1 1.57 us: per_device(): segment_overall = jnp.sum(log_decay, axis=0)]
    unnamed x7 -> x12, local copies, waits for them, and re-layouts: 3.15 us -> 5.38 us
  transfers between devices with their start and end apart: 4 -> 0, of which waited for: 3 -> 0; matrix products, arithmetic and copies ran while one was open for 11% -> 0% of each run, Pallas kernels for 0% -> 0%
where the time goes in v1:
time: 96 us; the launch traced here: 95.7 us
  Pallas kernels  89.6 us (93%)
  local copies, waits for them, and re-layouts  5.38 us (6%)
    pallas_call x1, Pallas kernels, per_device(): pl.pallas_call(kernel, out_shape=(jax.ShapeDtypeStruct((2, DV), BF16), ja...  89.6 us
    unnamed x12, local copies, waits for them, and re-layouts  5.38 us

profile of v1, /device:TPU:1, one launch (start us, length us, event | category | flops | bytes accessed | tf_op | source)
XLA Modules:
  0.0 95.7 jit_solution(4815253326765877602)
XLA Ops:
  0.6 1.5 %copy.8.lock_hbm = bf16[4096,64]{1,0:T(8,128)(2,1)S(1)} copy(bf16[4096,64]{0,1:T(8,128)(2,1)} %param.7) | data formatting | bytes 1048576 | tf_op args[1]
  2.2 0.0 copy-start
  2.2 0.0 copy-start.2
  2.2 0.0 copy-start.3
  2.2 1.6 %copy.9.dec_hbm = bf16[4096,64]{1,0:T(8,128)(2,1)S(1)} copy(bf16[4096,64]{0,1:T(8,128)(2,1)} %param.9) | data formatting | bytes 1048576 | tf_op args[3]
  3.8 0.0 copy-done
  3.8 0.0 copy-done.2
  3.8 0.0 copy-done.3
  3.8 0.0 copy-start.1
  3.8 1.2 %copy-done.1 = bf16[4096,128]{1,0:T(8,128)(2,1)S(1)} copy-done((bf16[4096,128]{1,0:T(8,128)(2,1)S(1)}, bf16[4096,128]{1,0:T(8,128)(2,1)}, u32[]{:S(2)}) %copy-start.1) | copy-done | bytes 1048600
  5.1 89.6 %shard_map.77 = (bf16[2,128]{1,0:T(2,128)(2,1)S(1)}, bf16[1,128]{1,0:T(2,128)(2,1)S(1)}) custom-call(bf16[128,4096]{1,0:T(8,128)(2,1)S(1)} %copy-done, bf16[4096,64]{1,0:T(8,128)(2,1)S(1)} %copy.8.lock_hbm, bf16[4096,128]{1,0:T(8,128)(2,1)S(1)} %copy-done.1, bf16[4096,64]{1,0:T(8,128)(2,1)S(1)} %copy.9.dec_hbm, f32[1,64]{1,0:T(1,128)S(1)} %bitcast.2, ...), custom_call_target="tpu_custom_call" | custom-call | tf_op jit(solution)/shard_map/pallas_call | solution.py:456
  94.7 0.5 copy.12
  95.2 0.5 copy.13
Async XLA Ops:
  2.2 1.6 %copy-start = (bf16[128,4096]{1,0:T(8,128)(2,1)S(1)}, bf16[128,4096]{1,0:T(8,128)(2,1)}, u32[]{:S(2)}) copy-start(bf16[128,4096]{1,0:T(8,128)(2,1)} %tok_hbm.1) | copy-start | bytes 3145732
  2.2 1.6 %copy-start.2 = (f32[64]{0:T(128)S(1)}, f32[64]{0:T(128)}, u32[]{:S(2)}) copy-start(f32[64]{0:T(128)} %param.10) | copy-start | bytes 772
  2.2 1.6 %copy-start.3 = (bf16[1,64]{1,0:T(2,128)(2,1)S(1)}, bf16[1,64]{1,0:T(2,128)(2,1)}, u32[]{:S(2)}) copy-start(bf16[1,64]{1,0:T(2,128)(2,1)} %q_ref.1) | copy-start | bytes 388
  3.8 1.2 %copy-start.1 = (bf16[4096,128]{1,0:T(8,128)(2,1)S(1)}, bf16[4096,128]{1,0:T(8,128)(2,1)}, u32[]{:S(2)}) copy-start(bf16[4096,128]{1,0:T(8,128)(2,1)} %val_hbm.1) | copy-start | bytes 3145732

commit v2 on v1

v2 whole, which is shorter than its diff:
```python
import math

import jax
import jax.numpy as jnp
from jax import lax
from jax.experimental import pallas as pl
from jax.experimental.pallas import tpu as pltpu
from jax.sharding import PartitionSpec as P

F32 = jnp.float32
BF16 = jnp.bfloat16
MESH = pl.DeviceIdType.MESH
NX, NY, NZ = 4, 8, 8
NSP = NX * NZ
D = 4096
CUE = 64
DV = 128
ROWS = 128
CHIP = 2 * ROWS
SLICE = D // NZ
HALF = SLICE // 2
TAU = 16.0
LN_LENGTH = math.log(65536)


def log_sigmoid(t):
    u = jnp.exp(-jnp.abs(t))
    s = u / (u + 2.0)
    s2 = s * s
    series = jnp.full_like(s, 1.0 / 17.0)
    for odd in (15, 13, 11, 9, 7, 5, 3, 1):
        series = series * s2 + 1.0 / odd
    return jnp.minimum(t, 0.0) - 2.0 * s * series


def kernel(
    tok_hbm, lock_hbm, val_hbm, dec_hbm, off_ref, q_ref,
    state_out, read_out,
    tok, w, wsrc, wfar, narrow, full, offsrc, offs, acc, after, kk, weighted,
    tot, t1, t2src, t2, st, s1, s2src, s2,
    load_sem, y_send, y_recv, o_send, o_recv, f_send, f_recv, z_send, z_recv, x_send, x_recv, d_send, d_recv,
    t1_send, t1_recv, t2_send, t2_recv, s1_send, s1_recv, s2_send, s2_recv,
    row_in, column_in, owner_in,
):
    sp = lax.axis_index("sp")
    tp = lax.axis_index("tp")
    z = sp // NX
    x = sp % NX
    y = tp // 2
    c = tp % 2

    def dev(x_, y_, z_, c_=None):
        return {"sp": z_ * NX + x_, "tp": y_ * 2 + (c if c_ is None else c_)}

    o = (x, 4 + (4 - x) % 4)
    up = [(y + o[s]) % NY for s in range(2)]
    down = [(y - o[s] + NY) % NY for s in range(2)]
    xr, xl = (x + 1) % NX, (x + 3) % NX
    zr, zl = (z + 1) % NZ, (z + 7) % NZ
    x2 = (x + 2) % NX
    mine = c * ROWS
    other = (1 - c) * ROWS

    zrow = pl.multiple_of(z * SLICE, SLICE)
    zfar = pl.multiple_of((z + 4) % NZ * SLICE, SLICE)
    loads = [
        pltpu.make_async_copy(lock_hbm.at[:, pl.ds(zrow, SLICE)], narrow.at[0:CUE], load_sem.at[0]),
        pltpu.make_async_copy(dec_hbm.at[:, pl.ds(zrow, SLICE)], narrow.at[CUE : 2 * CUE], load_sem.at[1]),
        pltpu.make_async_copy(val_hbm.at[pl.ds(zrow, SLICE)], wsrc.at[1], load_sem.at[2]),
        pltpu.make_async_copy(tok_hbm, tok.at[x, pl.ds(pl.multiple_of(mine, ROWS), ROWS)], load_sem.at[3]),
        pltpu.make_async_copy(val_hbm.at[pl.ds(zfar, SLICE)], wfar, load_sem.at[6]),
    ]
    for load in loads:
        load.start()
    own_loads = [
        pltpu.make_async_copy(lock_hbm, full.at[0:CUE], load_sem.at[4]),
        pltpu.make_async_copy(dec_hbm, full.at[CUE : 2 * CUE], load_sem.at[5]),
        pltpu.make_async_copy(val_hbm, w.at[1, :, 0:128], load_sem.at[7]),
    ]
    home = x == 0

    @pl.when(home)
    def _():
        for load in own_loads:
            load.start()

    barrier = pltpu.get_barrier_semaphore()

    def greet(device):
        pl.semaphore_signal(barrier, inc=1, device_id=device, device_id_type=MESH)

    greet(dev(x, y, z, 1 - c))
    for i in range(1, NX):
        greet(dev((x + i) % NX, y, z))
    for i in range(1, NY):
        greet(dev(x, (y + i) % NY, z))
    for i in range(1, NZ):
        greet(dev(x, y, (z + i) % NZ))

    def t1_peer(s, dy):
        yy = (y + dy) % NY
        d = (up[s] - yy + NY) % NY
        r = d // 4
        return (d + r * (8 - 2 * d)) % NX, yy, r

    lane = lax.broadcasted_iota(jnp.int32, (1, 128), 1)
    low = lane < CUE
    offsrc[...] = jnp.broadcast_to(jnp.concatenate([off_ref[...], off_ref[...]], axis=1), offsrc.shape)
    loads[0].wait()
    loads[1].wait()
    wsrc[0] = narrow[...].T
    loads[2].wait()
    loads[3].wait()

    pl.semaphore_wait(barrier, 1 + NX - 1 + NY - 1 + NZ - 1)

    def tell(sem, device):
        pl.semaphore_signal(sem, inc=1, device_id=device, device_id_type=MESH)

    for i in range(1, NY):
        tell(row_in, dev(x, (y + i) % NY, z))
    for i in range(1, NX):
        tell(column_in, dev((x + i) % NX, y, z))
    tell(owner_in, dev(x, down[1], z))

    def remote(src, dst, send, recv, device):
        return pltpu.make_async_remote_copy(
            src_ref=src, dst_ref=dst, send_sem=send, recv_sem=recv, device_id=device, device_id_type=MESH
        )

    def y_copy(s, k):
        t, j = k // 2, k % 2
        rows = pl.ds(pl.multiple_of(z * SLICE + j * HALF, HALF), HALF)
        return remote(
            wsrc.at[t, pl.ds(j * HALF, HALF)],
            w.at[t, rows, pl.ds(s * 128, 128)],
            y_send.at[s, k], y_recv.at[s, k], dev(x, down[s], z),
        )

    def o_copy(s):
        return remote(offsrc, offs.at[s], o_send.at[s], o_recv.at[s], dev(x, down[s], z))

    def far_copy(s):
        return remote(
            wfar, w.at[1, pl.ds(zfar, SLICE), pl.ds(s * 128, 128)],
            f_send.at[s], f_recv.at[s], dev(x, down[s], z),
        )

    def abroad(action):
        pl.when(jnp.logical_not(home))(action)

    def y_start(k):
        y_copy(1, k).start()
        abroad(lambda: y_copy(0, k).start())

    def y_left(k):
        y_copy(1, k).wait_send()
        abroad(lambda: y_copy(0, k).wait_send())

    def far_start():
        @abroad
        def _():
            for s in range(2):
                far_copy(s).start()

    y_start(0)

    def x_rows(direction, p):
        piece = (p % 4 + 2 * direction) % 4 if p < 4 else p - 4 + 2 * direction
        return pl.ds(pl.multiple_of(mine + piece * 32, 32), 32)

    def x_copy(direction, p):
        owner = x if p < 4 else (xl if direction == 0 else xr)
        ref = tok.at[owner, x_rows(direction, p)]
        return remote(ref, ref, x_send.at[direction, p], x_recv.at[direction, p],
                      dev(xr if direction == 0 else xl, y, z))

    for p in range(4):
        for direction in range(2):
            x_copy(direction, p).start()

    def d_copy(direction, p):
        if p < 0:
            ref, n = tok.at[x, pl.ds(pl.multiple_of(mine, ROWS), ROWS)], 12
        else:
            owner = x2 if p > 3 else (xl if direction == 0 else xr)
            ref, n = tok.at[owner, x_rows(direction, p)], 2 * p + direction
        return remote(ref, ref, d_send.at[n], d_recv.at[n], dev(x, y, z, 1 - c))

    d_copy(0, -1).start()

    def pieces_in(p):
        for direction in range(2):
            x_copy(direction, p).wait_recv()
            d_copy(direction, p).start()
            if p < 2:
                x_copy(direction, p + 4).start()

    def pieces_across(first, count):
        for p in range(first, first + count):
            for direction in range(2):
                d_copy(direction, p).wait_recv()

    def z_ref(s, direction, k, d, hop):
        t, j = k // 2, k % 2
        owner = (z - d + NZ) % NZ if direction == 0 else (z + d) % NZ
        start, size = owner * SLICE + j * HALF, HALF
        if hop == 3:
            start, size = start + direction * (HALF // 2), HALF // 2
        return w.at[t, pl.ds(pl.multiple_of(start, HALF // 2), size), pl.ds(s * 128, 128)]

    def z_copy(s, direction, k, d):
        ref = z_ref(s, direction, k, d, d)
        return remote(ref, ref, z_send.at[s, direction, k, d], z_recv.at[s, direction, k, d],
                      dev(x, y, zr if direction == 0 else zl))

    def z_wait(s, direction, k, d):
        ref = z_ref(s, direction, k, d + 1, d)
        remote(ref, ref, z_send.at[s, direction, k, d], z_recv.at[s, direction, k, d], dev(x, y, zr)).wait_recv()

    def each_slot(action):
        abroad(lambda: action(0))
        action(1)

    def own(k):
        def send(s):
            y_copy(s, k).wait_recv()
            for direction in range(2):
                z_copy(s, direction, k, 0).start()

        each_slot(send)

    def hop(k, d):
        def forward(s):
            for direction in range(2):
                z_wait(s, direction, k, d - 1)
                z_copy(s, direction, k, d).start()

        each_slot(forward)

    def third(k):
        @abroad
        def _():
            for s in range(2):
                for direction in range(2):
                    z_wait(s, direction, k, 2)

    def third_home(k):
        @pl.when(home)
        def _():
            for direction in range(2):
                z_wait(1, direction, k, 2)
                z_copy(1, direction, k, 3).start()

    def last_keys():
        def arrive(s):
            for k in range(2):
                for direction in range(2):
                    z_wait(s, direction, k, 3)

        each_slot(arrive)

    def last_values():
        @abroad
        def _():
            for s in range(2):
                far_copy(s).wait_recv()

        @pl.when(home)
        def _():
            for k in (2, 3):
                for direction in range(2):
                    z_wait(1, direction, k, 3)

    def keys(offset, first=False):
        cols = pl.ds(pl.multiple_of((z + offset) % NZ * SLICE, SLICE), SLICE)
        w_piece = w[0, cols]
        for block in (x, xr, xl):
            term = jnp.dot(tok[block, :, cols], w_piece, preferred_element_type=F32)
            out = pl.ds(pl.multiple_of(block * CHIP, CHIP), CHIP)
            acc[0, out] = term if first else acc[0, out] + term

    def part(i):
        starts = [j * 64 + i * 32 for j in range(4)]
        rows = jnp.concatenate([tok[x2, start : start + 32] for start in starts], axis=0)
        product = jnp.dot(rows, w[0], preferred_element_type=F32)
        for j, start in enumerate(starts):
            out = pl.ds(pl.multiple_of(x2 * CHIP + start, 32), 32)
            acc[0, out] = product[j * 32 : j * 32 + 32]

    def values(offset, first=False):
        cols = pl.ds(pl.multiple_of((z + offset) % NZ * SLICE, SLICE), SLICE)
        w_piece = w[1, cols]
        for b in range(NX):
            term = jnp.dot(tok[b, :, cols], w_piece, preferred_element_type=F32)
            out = pl.ds(b * CHIP, CHIP)
            acc[1, out] = term if first else acc[1, out] + term

    y_left(0)
    y_start(1)
    loads[4].wait()

    @pl.when(home)
    def _():
        for load in own_loads:
            load.wait()
        for i in range(NZ):
            w[0, i * SLICE : (i + 1) * SLICE, 0:128] = full[:, i * SLICE : (i + 1) * SLICE].T
        offs[0] = offsrc[...]

    @abroad
    def _():
        o_copy(0).start()

    o_copy(1).start()
    own(0)
    pieces_in(0)
    own(1)
    y_start(2)
    y_start(3)

    o_copy(1).wait_recv()

    @pl.when(x != 0)
    def _():
        o_copy(0).wait_recv()

    offset = jnp.where(low, offs[0, 0:1], offs[1, 0:1])
    later_rows = (
        lax.broadcasted_iota(jnp.int32, (CHIP, CHIP), 1) > lax.broadcasted_iota(jnp.int32, (CHIP, CHIP), 0)
    ).astype(BF16)

    def decay(b):
        rows = pl.ds(pl.multiple_of(b * CHIP, CHIP), CHIP)
        first, second = acc[0, rows, 0:128], acc[0, rows, 128:256]
        kk[rows] = jnp.where(low, first, pltpu.roll(second, CUE, 1)).astype(BF16)
        pre = jnp.where(low, pltpu.roll(first, CUE, 1), second)
        log_decay = log_sigmoid(pre + offset + LN_LENGTH) * (1.0 / TAU)
        high = log_decay.astype(BF16)
        rest = log_decay - high.astype(F32)
        middle = rest.astype(BF16)
        small = (rest - middle.astype(F32)).astype(BF16)
        sums = jnp.dot(later_rows, jnp.concatenate([high, middle, small], axis=1), preferred_element_type=F32)
        local = sums[:, 256:384] + sums[:, 128:256] + sums[:, 0:128]
        after[rows] = local
        total = local[0:1] + log_decay[0:1]
        tot[0, b] = total
        tot[1, b] = pltpu.roll(total, CUE, 1)


    hop(0, 1)
    pieces_in(1)
    hop(1, 1)
    hop(0, 2)
    hop(1, 2)
    far_start()
    pieces_in(2)
    hop(0, 3)
    own(2)
    hop(1, 3)
    own(3)
    pieces_in(3)
    d_copy(0, -1).wait_recv()
    pieces_across(0, 4)
    keys(0, True)
    keys(1)
    keys(NZ - 1)
    keys(2)
    keys(NZ - 2)
    last_keys()
    hop(2, 1)
    keys(3)
    keys(NZ - 3)
    keys(4)
    pieces_in(4)
    decay(x)
    decay(xr)
    decay(xl)
    pieces_across(4, 1)
    part(0)
    hop(3, 1)
    pieces_in(5)
    pieces_across(5, 1)
    part(1)
    decay(x2)

    def t1_copy(s, dy):
        xx, yy, r = t1_peer(s, dy)
        differs = (r + s) % 2
        return remote(tot.at[differs], t1.at[r, y], t1_send, t1_recv, dev(xx, yy, z))

    def t1_start(dy, carry):
        for s in range(2):
            t1_copy(s, dy).start()
        return carry

    pl.semaphore_wait(row_in, NY - 1)
    lax.fori_loop(1, NY, t1_start, 0)
    for s in range(2):
        t1[s, y] = tot[0]

    hop(2, 2)

    values(0, True)
    hop(3, 2)
    third_home(2)
    third_home(3)
    values(1)
    values(NZ - 1)

    t1_bytes = t1.at[:, 0 : NY - 1]
    remote(t1_bytes, t1_bytes, t1_send, t1_recv, dev(x, y, z, 1 - c)).wait_recv()
    blocks = jnp.where(low[None, None], t1[0], t1[1])
    per_x = jnp.sum(blocks, axis=0)
    y_index = lax.broadcasted_iota(jnp.int32, blocks.shape, 0)
    later_y = jnp.sum(jnp.where(y_index > y, blocks, 0.0), axis=0)
    t2src[...] = per_x[0] + per_x[1] + per_x[2] + per_x[3]

    def t2_copy(i):
        return remote(t2src, t2.at[z], t2_send, t2_recv, dev(x, up[1], (z + i) % NZ))

    def t2_start(i, carry):
        t2_copy(i).start()
        return carry

    pl.semaphore_wait(owner_in, 1)
    lax.fori_loop(1, NZ, t2_start, 0)
    t2[z] = jnp.zeros_like(t2src)

    later = jnp.zeros((1, 128), F32)
    for b in range(NX - 1, -1, -1):
        rows = pl.ds(b * CHIP, CHIP)
        factor = jnp.exp(after[rows] + (later + later_y[b]))
        weighted[rows] = (kk[rows].astype(F32) * factor).astype(BF16)
        later = later + per_x[b]

    values(2)
    values(NZ - 2)
    last_values()
    values(4)
    third(2)
    third(3)
    values(3)
    values(NZ - 3)

    state = lax.dot_general(
        weighted[...], acc[1].astype(BF16), (((0,), (0,)), ((), ())), preferred_element_type=F32
    )
    st[0] = state[0:CUE, 0:DV]
    st[1] = state[CUE:, DV:]

    def s1_copy(s):
        return remote(st.at[s], s1.at[s], s1_send.at[s], s1_recv.at[s], dev(x, up[s], z))

    s1_copy(1).start()

    @pl.when(x != 0)
    def _():
        s1_copy(0).start()

    @pl.when(x == 0)
    def _():
        s1[0] = state[0:CUE, 0:DV]

    eye = (
        lax.broadcasted_iota(jnp.int32, (CUE, CUE), 0) == lax.broadcasted_iota(jnp.int32, (CUE, CUE), 1)
    )
    question = jnp.sum(jnp.where(eye, q_ref[...].astype(F32), 0.0), axis=1, keepdims=True) * CUE ** -0.5

    s1_copy(1).wait_recv()

    @pl.when(x != 0)
    def _():
        s1_copy(0).wait_recv()

    t2_bytes = t2.at[0 : NZ - 1]
    remote(t2_bytes, t2_bytes, t2_send, t2_recv, dev(x, y, z, 1 - c)).wait_recv()
    spans = t2[...]
    z_index = lax.broadcasted_iota(jnp.int32, spans.shape, 0)
    later_z = jnp.exp(jnp.sum(jnp.where(z_index > z, spans, 0.0), axis=0))[:, CUE:]
    kept = jnp.sum(jnp.where(eye, later_z, 0.0), axis=1, keepdims=True)
    summed = (s1[0] + s1[1]) * kept
    term = jnp.sum(question * summed, axis=0, keepdims=True)
    s2src[:, 0:2] = summed.reshape(NSP, 2, DV)
    s2src[:, 2:4] = jnp.broadcast_to(term[None], (NSP, 2, DV))

    def s2_copy(i):
        peer = (sp + i) % NSP
        return remote(s2src.at[peer], s2.at[sp], s2_send, s2_recv, {"sp": peer, "tp": tp})

    def s2_start(i, carry):
        s2_copy(i).start()
        return carry

    pl.semaphore_wait(column_in, NX - 1)
    lax.fori_loop(1, NSP, s2_start, 0)
    s2[sp] = s2src[sp]
    s2_bytes = s2.at[0 : NSP - 1]
    remote(s2_bytes, s2_bytes, s2_send, s2_recv, dev(x, y, z, 1 - c)).wait_recv()
    total = jnp.sum(s2[...], axis=0)
    state_out[...] = total[0:2].astype(BF16)
    heard = total[2:3]
    square = jnp.mean(heard * heard, axis=1, keepdims=True)
    read_out[...] = (heard * lax.rsqrt(square + 1.0)).astype(BF16)

    for k in range(1, 4):
        y_left(k)

    def z_left(s):
        for k in range(4):
            for d in range(3):
                for direction in range(2):
                    z_copy(s, direction, k, d).wait_send()

    each_slot(z_left)
    o_copy(1).wait_send()
    s1_copy(1).wait_send()

    @pl.when(home)
    def _():
        for k in range(4):
            for direction in range(2):
                z_copy(1, direction, k, 3).wait_send()

    @abroad
    def _():
        o_copy(0).wait_send()
        s1_copy(0).wait_send()
        for s in range(2):
            far_copy(s).wait_send()
            for k in range(2):
                for direction in range(2):
                    z_copy(s, direction, k, 3).wait_send()

    d_copy(0, -1).wait_send()
    for p in range(6):
        for direction in range(2):
            x_copy(direction, p).wait_send()
            d_copy(direction, p).wait_send()
    remote(t1_bytes, t1_bytes, t1_send, t1_recv, dev(x, y, z, 1 - c)).wait_send()
    remote(t2_bytes, t2_bytes, t2_send, t2_recv, dev(x, y, z, 1 - c)).wait_send()
    remote(s2_bytes, s2_bytes, s2_send, s2_recv, dev(x, y, z, 1 - c)).wait_send()


def per_device(tokens, lock_projector, value_weight, decay_weight, decay_offset, fresh_question):
    dma = pltpu.SemaphoreType.DMA
    signal = pltpu.SemaphoreType.REGULAR
    anywhere = pl.BlockSpec(memory_space=pl.ANY)
    vmem = pl.BlockSpec(memory_space=pltpu.VMEM)
    state, read = pl.pallas_call(
        kernel,
        out_shape=(jax.ShapeDtypeStruct((2, DV), BF16), jax.ShapeDtypeStruct((1, DV), BF16)),
        in_specs=[anywhere] * 4 + [vmem] * 2,
        out_specs=(vmem, vmem),
        scratch_shapes=[
            pltpu.VMEM((NX, CHIP, D), BF16),
            pltpu.VMEM((2, D, 256), BF16),
            pltpu.VMEM((2, SLICE, 128), BF16),
            pltpu.VMEM((SLICE, 128), BF16),
            pltpu.VMEM((2 * CUE, SLICE), BF16),
            pltpu.VMEM((2 * CUE, D), BF16),
            pltpu.VMEM((8, 128), F32),
            pltpu.VMEM((2, 8, 128), F32),
            pltpu.VMEM((2, NX * CHIP, 256), F32),
            pltpu.VMEM((NX * CHIP, 128), F32),
            pltpu.VMEM((NX * CHIP, 128), BF16),
            pltpu.VMEM((NX * CHIP, 128), BF16),
            pltpu.VMEM((2, NX, 1, 128), F32),
            pltpu.VMEM((2, NY, NX, 1, 128), F32),
            pltpu.VMEM((1, 128), F32),
            pltpu.VMEM((NZ, 1, 128), F32),
            pltpu.VMEM((2, CUE, DV), F32),
            pltpu.VMEM((2, CUE, DV), F32),
            pltpu.VMEM((NSP, 4, DV), F32),
            pltpu.VMEM((NSP, 4, DV), F32),
            dma((8,)),
            dma((2, 4)), dma((2, 4)),
            dma((2,)), dma((2,)),
            dma((2,)), dma((2,)),
            dma((2, 2, 4, 4)), dma((2, 2, 4, 4)),
            dma((2, 6)), dma((2, 6)),
            dma((13,)), dma((13,)),
            dma, dma,
            dma, dma,
            dma((2,)), dma((2,)),
            dma, dma,
            signal, signal, signal,
        ],
        compiler_params=pltpu.CompilerParams(
            collective_id=0, has_side_effects=True, vmem_limit_bytes=55000 * 1024
        ),
    )(
        tokens, lock_projector.T, value_weight, decay_weight.T,
        decay_offset.reshape(1, CUE), fresh_question,
    )
    return state.reshape(1, 2, DV), read


def solution(mesh):
    in_specs = (
        P(("sp", "tp"), None),
        P(None, "tp"),
        P(None, "tp"),
        P(None, "tp"),
        P("tp"),
        P("tp", None),
    )
    out_specs = (P("tp", "sp", None), P("tp", None))
    return jax.shard_map(
        per_device, mesh=mesh, in_specs=in_specs, out_specs=out_specs, check_vma=False
    )
```

time: 96 us -> 79.3 us (0.83)
  the two profiles are of different devices: /device:TPU:1 before, /device:TPU:48 now
where the time goes in v2:
time: 79.3 us; the launch traced here: 79.2 us
  Pallas kernels  76.8 us (97%)
  local copies, waits for them, and re-layouts  1.68 us (2%)
    pallas_call x1, Pallas kernels, per_device(): pl.pallas_call(kernel, out_shape=(jax.ShapeDtypeStruct((2, DV), BF16), ja...  76.8 us
    unnamed x6, local copies, waits for them, and re-layouts  1.68 us

profile of v2, /device:TPU:48, one launch (start us, length us, event | category | flops | bytes accessed | tf_op | source)
XLA Modules:
  0.0 79.2 jit_solution(10986283293491488491)
XLA Ops:
  0.6 0.0 copy-start
  0.6 0.0 copy-start.1
  0.7 0.6 copy-done
  1.3 0.0 copy-done.1
  1.3 76.8 %shard_map.77 = (bf16[2,128]{1,0:T(2,128)(2,1)S(1)}, bf16[1,128]{1,0:T(2,128)(2,1)S(1)}) custom-call(bf16[128,4096]{1,0:T(8,128)(2,1)} %tok_hbm.1, bf16[64,4096]{1,0:T(8,128)(2,1)} %bitcast.6, bf16[4096,128]{1,0:T(8,128)(2,1)} %val_hbm.1, bf16[64,4096]{1,0:T(8,128)(2,1)} %bitcast.7, f32[1,64]{1,0:T(1,128)S(1)} %bitcast.4, bf16[1,64]{1,0:T(2,128)(2,1)S(1)} %copy-done.1), custom_call_target="tpu_custom_call" | custom-call | tf_op jit(solution)/shard_map/pallas_call | solution.py:550
  78.1 0.5 copy.10
  78.7 0.5 copy.11
Async XLA Ops:
  0.6 0.7 copy-start
  0.6 0.7 copy-start.1

commit v3 on v0

v3 whole, which is shorter than its diff:
```python
import math

import jax
import jax.numpy as jnp
from jax import lax
from jax.experimental import pallas as pl
from jax.experimental.pallas import tpu as pltpu
from jax.sharding import PartitionSpec as P

F32 = jnp.float32
BF16 = jnp.bfloat16
MESH = pl.DeviceIdType.MESH
NX, NY, NZ = 4, 8, 8
NSP = NX * NZ
D = 4096
CUE = 64
DV = 128
ROWS = 128
CHIP = 2 * ROWS
SLICE = D // NZ
HALF = SLICE // 2
TAU = 16.0
LN_LENGTH = math.log(65536)
PIECES = ((0, 48), (48, 16))


def log_sigmoid(t):
    u = jnp.exp(-jnp.abs(t))
    s = u / (u + 2.0)
    s2 = s * s
    series = jnp.full_like(s, 1.0 / 17.0)
    for odd in (15, 13, 11, 9, 7, 5, 3, 1):
        series = series * s2 + 1.0 / odd
    return jnp.minimum(t, 0.0) - 2.0 * s * series


def kernel(
    tok_hbm, lock_hbm, val_hbm, dec_hbm, off_ref, q_ref,
    state_out, read_out,
    tok, w, wsrc, wfar, narrow, full, offsrc, offs, acc, after, kk, weighted,
    tot, t1, t2src, t2, later_in_z, question, ssrc, sdst,
    load_sem, y_send, y_recv, o_send, o_recv, f_send, f_recv, z_send, z_recv, x_send, x_recv, d_send, d_recv,
    t1_send, t1_recv, t2_send, t2_recv, s_send, s_recv,
    row_in, column_in, plane_in,
):
    sp = lax.axis_index("sp")
    tp = lax.axis_index("tp")
    z = sp // NX
    x = sp % NX
    y = tp // 2
    c = tp % 2

    def dev(x_, y_, z_, c_=None):
        return {"sp": z_ * NX + x_, "tp": y_ * 2 + (c if c_ is None else c_)}

    near = (x + 4 * (x // 3)) % NY
    o = (near, (near + 4) % NY)
    up = [(y + o[s]) % NY for s in range(2)]
    down = [(y - o[s] + NY) % NY for s in range(2)]
    xr, xl = (x + 1) % NX, (x + 3) % NX
    zr, zl = (z + 1) % NZ, (z + 7) % NZ
    mine = c * ROWS
    other = (1 - c) * ROWS

    zrow = pl.multiple_of(z * SLICE, SLICE)
    zfar = pl.multiple_of((z + 4) % NZ * SLICE, SLICE)
    loads = [
        pltpu.make_async_copy(lock_hbm.at[:, pl.ds(zrow, SLICE)], narrow.at[0:CUE], load_sem.at[0]),
        pltpu.make_async_copy(dec_hbm.at[:, pl.ds(zrow, SLICE)], narrow.at[CUE : 2 * CUE], load_sem.at[0]),
        pltpu.make_async_copy(val_hbm.at[pl.ds(zrow, SLICE)], wsrc.at[1], load_sem.at[1]),
        pltpu.make_async_copy(tok_hbm, tok.at[0, pl.ds(pl.multiple_of(mine, ROWS), ROWS)], load_sem.at[2]),
        pltpu.make_async_copy(val_hbm.at[pl.ds(zfar, SLICE)], wfar, load_sem.at[3]),
    ]
    for load in loads:
        load.start()
    own_loads = [
        pltpu.make_async_copy(lock_hbm, full.at[0:CUE], load_sem.at[4]),
        pltpu.make_async_copy(dec_hbm, full.at[CUE : 2 * CUE], load_sem.at[4]),
        pltpu.make_async_copy(val_hbm, w.at[1, :, 0:128], load_sem.at[4]),
    ]
    home = x == 0

    @pl.when(home)
    def _():
        for load in own_loads:
            load.start()

    barrier = pltpu.get_barrier_semaphore()

    def greet(device):
        pl.semaphore_signal(barrier, inc=1, device_id=device, device_id_type=MESH)

    greet(dev(x, y, z, 1 - c))
    for i in range(1, NX):
        greet(dev((x + i) % NX, y, z))
    for i in range(1, NY):
        greet(dev(x, (y + i) % NY, z))
    greet(dev(x, y, zr))
    greet(dev(x, y, zl))

    def t1_peer(s, dy):
        yy = (y + dy) % NY
        d = (up[s] - yy + NY) % NY
        xx = d % NX
        return xx, yy, (d // NX + xx // 3) % 2

    lane = lax.broadcasted_iota(jnp.int32, (1, 128), 1)
    low = lane < CUE
    packed = jnp.concatenate([off_ref[...], q_ref[...].astype(F32)], axis=0)
    offsrc[...] = jnp.concatenate([packed, packed], axis=1)
    pltpu.make_async_copy(narrow, narrow, load_sem.at[0]).wait()
    wsrc[0] = narrow[...].T
    loads[2].wait()
    loads[3].wait()

    pl.semaphore_wait(barrier, 1 + NX - 1 + NY - 1 + 2)

    def tell(sem, device):
        pl.semaphore_signal(sem, inc=1, device_id=device, device_id_type=MESH)

    for i in range(1, NY):
        tell(row_in, dev(x, (y + i) % NY, z))

    def remote(src, dst, send, recv, device):
        return pltpu.make_async_remote_copy(
            src_ref=src, dst_ref=dst, send_sem=send, recv_sem=recv, device_id=device, device_id_type=MESH
        )

    def y_copy(s, k):
        t, j = k // 2, k % 2
        rows = pl.ds(pl.multiple_of(z * SLICE + j * HALF, HALF), HALF)
        return remote(
            wsrc.at[t, pl.ds(j * HALF, HALF)],
            w.at[t, rows, pl.ds(s * 128, 128)],
            y_send.at[min(k, 1)], y_recv.at[s, k], dev(x, down[s], z),
        )

    def o_copy(s):
        return remote(offsrc, offs.at[s], o_send, o_recv, dev(x, down[s], z))

    def far_copy(s):
        return remote(
            wfar, w.at[1, pl.ds(zfar, SLICE), pl.ds(s * 128, 128)],
            f_send, f_recv, dev(x, down[s], z),
        )

    def abroad(action):
        pl.when(jnp.logical_not(home))(action)

    y_copy(1, 0).start()
    abroad(lambda: y_copy(0, 0).start())

    def x_rows(direction, p):
        half = direction if p in (0, 1, 4, 5) else 1 - direction
        start, size = PIECES[p % 2]
        return pl.ds(pl.multiple_of(mine + half * 64 + start, 16), size)

    def x_copy(direction, p):
        rows = x_rows(direction, p)
        side = (2, 1)[direction]
        source, target = (0, side) if p < 4 else (side, 3)
        return remote(tok.at[source, rows], tok.at[target, rows], x_send, x_recv.at[p],
                      dev((xr, xl)[direction], y, z))

    for p in range(4):
        for direction in range(2):
            x_copy(direction, p).start()

    def d_copy(direction, p):
        if p < 0:
            ref, n = tok.at[0, pl.ds(pl.multiple_of(mine, ROWS), ROWS)], 6
        else:
            ref, n = tok.at[3 if p > 3 else (2, 1)[direction], x_rows(direction, p)], p
        return remote(ref, ref, d_send, d_recv.at[n], dev(x, y, z, 1 - c))

    d_copy(0, -1).start()

    def token_rows(rows):
        return tok.at[0, 0:rows]

    def pieces_in(p):
        ref = token_rows(2 * PIECES[p % 2][1])
        remote(ref, ref, x_send, x_recv.at[p], dev(xr, y, z)).wait_recv()
        for direction in range(2):
            d_copy(direction, p).start()
            if p < 2:
                x_copy(direction, p + 4).start()

    def pieces_across(first, count):
        for p in range(first, first + count):
            ref = token_rows(2 * PIECES[p % 2][1])
            remote(ref, ref, d_send, d_recv.at[p], dev(x, y, z, 1 - c)).wait_recv()

    def z_ref(s, direction, k, d, hop):
        t, j = k // 2, k % 2
        owner = (z - d + NZ) % NZ if direction == 0 else (z + d) % NZ
        start, size = owner * SLICE + j * HALF, HALF
        if hop == 3:
            start, size = start + direction * (HALF // 2), HALF // 2
        return w.at[t, pl.ds(pl.multiple_of(start, HALF // 2), size), pl.ds(s * 128, 128)]

    def z_copy(s, direction, k, d):
        ref = z_ref(s, direction, k, d, d)
        return remote(ref, ref, z_send, z_recv.at[s, k, d], dev(x, y, zr if direction == 0 else zl))

    def weight_rows(rows):
        return w.at[0, 0 : rows // 2] if rows <= 2 * D else w.at[:, 0 : rows // 4]

    def z_wait(s, k, d):
        ref = weight_rows(HALF if d == 3 else 2 * HALF)
        remote(ref, ref, z_send, z_recv.at[s, k, d], dev(x, y, zr)).wait_recv()

    def project(t, offset, first_block, blocks, fresh=False, start=0, size=SLICE):
        cols = pl.ds(pl.multiple_of((z + offset) % NZ * SLICE + start, HALF), size)
        rows = tok[first_block : first_block + blocks, :, cols].reshape(blocks * CHIP, size)
        term = jnp.dot(rows, w[t, cols], preferred_element_type=F32)
        out = pl.ds(first_block * CHIP, blocks * CHIP)
        acc[t, out] = term if fresh else acc[t, out] + term

    def keys(offset, fresh=False):
        project(0, offset, 0, NX - 1, fresh)

    def far_keys(offset, fresh=False):
        project(0, offset, NX - 1, 1, fresh)

    def values(offset, fresh=False, start=0, size=SLICE):
        project(1, offset, 0, NX, fresh, start, size)

    later_rows = (
        lax.broadcasted_iota(jnp.int32, (CHIP, CHIP), 1) > lax.broadcasted_iota(jnp.int32, (CHIP, CHIP), 0)
    ).astype(BF16)

    place = [(x + b) % NX for b in (0, 1, 3, 2)]

    def decay(b):
        offset = jnp.where(low, offs[0, 0:1], offs[1, 0:1])
        rows = pl.ds(b * CHIP, CHIP)
        pre = jnp.where(low, pltpu.roll(acc[0, rows, 0:128], CUE, 1), acc[0, rows, 128:256])
        log_decay = log_sigmoid(pre + offset + LN_LENGTH) * (1.0 / TAU)
        after[rows] = log_decay
        total = jnp.sum(log_decay, axis=0, keepdims=True)
        tot[0, place[b]] = total
        tot[1, place[b]] = pltpu.roll(total, CUE, 1)

    def suffix(b):
        rows = pl.ds(b * CHIP, CHIP)
        kk[rows] = jnp.where(low, acc[0, rows, 0:128], pltpu.roll(acc[0, rows, 128:256], CUE, 1)).astype(BF16)
        log_decay = after[rows]
        high = log_decay.astype(BF16)
        rest = log_decay - high.astype(F32)
        middle = rest.astype(BF16)
        small = (rest - middle.astype(F32)).astype(BF16)
        sums = jnp.dot(later_rows, jnp.concatenate([high, middle, small], axis=1), preferred_element_type=F32)
        after[rows] = sums[:, 256:384] + sums[:, 128:256] + sums[:, 0:128]

    def t1_copy(s, dy):
        xx, yy, r = t1_peer(s, dy)
        differs = (r + s) % 2
        return remote(tot.at[differs], t1.at[r, y], t1_send, t1_recv, dev(xx, yy, z))

    def t1_begin():
        pl.semaphore_wait(row_in, NY - 1)
        for dy in (4, 3, 5, 2, 6, 1, 7):
            for s in range(2):
                t1_copy(s, dy).start()
        for s in range(2):
            t1[s, y] = tot[0]

    t1_bytes = t1.at[:, 0 : NY - 1]
    t1_all = remote(t1_bytes, t1_bytes, t1_send, t1_recv, dev(x, y, z, 1 - c))

    def t2_copy(i):
        return remote(t2src, t2.at[z], t2_send, t2_recv, dev(x, y, (z + i) % NZ))

    t2_bytes = t2.at[0 : NZ - 1]
    t2_all = remote(t2_bytes, t2_bytes, t2_send, t2_recv, dev(x, y, z, 1 - c))

    def t1_end():
        t1_all.wait_recv()
        blocks = jnp.where(low[None, None], t1[0], t1[1])
        per_x = jnp.sum(blocks, axis=0)
        t2src[...] = per_x[0] + per_x[1] + per_x[2] + per_x[3]
        for i in (4, 3, 5, 2, 6, 1, 7):
            t2_copy(i).start()
        t2[z] = t2src[...]
        y_index = lax.broadcasted_iota(jnp.int32, blocks.shape, 0)
        later_y = jnp.sum(jnp.where(y_index > y, blocks, 0.0), axis=0)
        later = jnp.zeros((1, 128), F32)
        for b in range(NX - 1, -1, -1):
            later_in_z[b] = later + later_y[b]
            later = later + per_x[b]

    def t2_end():
        t2_all.wait_recv()
        spans = t2[...]
        z_index = lax.broadcasted_iota(jnp.int32, spans.shape, 0)
        later = jnp.sum(jnp.where(z_index > z, spans, 0.0), axis=0)
        for b in range(NX):
            rows = pl.ds(b * CHIP, CHIP)
            factor = jnp.exp(after[rows] + (later + later_in_z[place[b]]))
            weighted[rows] = (kk[rows].astype(F32) * factor).astype(BF16)
        eye = (
            lax.broadcasted_iota(jnp.int32, (128, 128), 0) == lax.broadcasted_iota(jnp.int32, (128, 128), 1)
        )
        asked = jnp.where(low, offs[0, 1:2], offs[1, 1:2]) * CUE ** -0.5
        column = jnp.sum(jnp.where(eye, asked, 0.0), axis=1, keepdims=True)
        question[...] = jnp.broadcast_to(column, question.shape)

    def flow(is_home):
        slots = (1,) if is_home else (0, 1)

        def y_start(k):
            for s in slots:
                y_copy(s, k).start()

        def own(k):
            for s in slots:
                y_copy(s, k).wait_recv()
                for direction in range(2):
                    z_copy(s, direction, k, 0).start()

        def hop(k, d):
            for s in slots:
                z_wait(s, k, d - 1)
                for direction in range(2):
                    z_copy(s, direction, k, d).start()

        def last(k):
            for s in slots:
                z_wait(s, k, 3)

        ref = weight_rows(HALF * len(slots))
        remote(ref, ref, y_send.at[0], y_recv.at[1, 0], dev(x, y, zr)).wait_send()
        y_start(1)
        for s in slots:
            o_copy(s).start()
        loads[4].wait()
        if is_home:
            pltpu.make_async_copy(w.at[0], w.at[0], load_sem.at[4]).wait()
            for i in range(NZ):
                w[0, i * SLICE : (i + 1) * SLICE, 0:128] = full[:, i * SLICE : (i + 1) * SLICE].T
            offs[0] = offsrc[...]
        own(0)
        if is_home:
            y_start(2)
            y_start(3)
        own(1)
        if not is_home:
            y_start(2)
            y_start(3)
        hop(0, 1)
        hop(1, 1)
        hop(0, 2)
        pieces_in(0)
        pieces_in(1)
        hop(1, 2)
        if not is_home:
            for s in slots:
                far_copy(s).start()
        hop(0, 3)
        own(2)
        hop(1, 3)
        own(3)
        offs_in = offs.at[0 : len(slots)]
        remote(offs_in, offs_in, o_send, o_recv, dev(x, y, zr)).wait_recv()
        pieces_in(2)
        pieces_in(3)
        d_copy(0, -1).wait_recv()
        pieces_across(0, 4)
        keys(0, True)
        keys(1)
        keys(NZ - 1)
        keys(2)
        keys(NZ - 2)
        last(0)
        hop(2, 1)
        last(1)
        for i in range(1, NX):
            tell(column_in, dev((x + i) % NX, y, z))
        keys(3)
        keys(NZ - 3)
        keys(4)
        hop(3, 1)
        pieces_in(4)
        pieces_in(5)
        if is_home:
            hop(2, 2)
        decay(0)
        decay(1)
        decay(2)
        if is_home:
            hop(3, 2)
        pieces_across(4, 2)
        for offset in range(NZ):
            far_keys(offset, offset == 0)
        decay(3)
        t1_begin()
        pl.semaphore_wait(column_in, NX - 1)
        for s in slots:
            tell(plane_in, dev(x, down[s], z))
        if not is_home:
            hop(2, 2)
        for b in range(NX):
            suffix(b)
        if not is_home:
            hop(3, 2)
        values(0, True)
        if is_home:
            hop(2, 3)
            hop(3, 3)
        values(1)
        values(NZ - 1)
        t1_end()
        values(2)
        values(NZ - 2)
        if is_home:
            values(3)
            values(NZ - 3)
            t2_end()
            for k in (2, 3):
                z_wait(1, k, 3)
            values(4)
        else:
            ref = weight_rows(2 * SLICE)
            remote(ref, ref, f_send, f_recv, dev(x, y, zr)).wait_recv()
            values(4)
            for k in (2, 3):
                if k == 3:
                    t2_end()
                for s in slots:
                    z_wait(s, k, 2)
                values(3, False, (k - 2) * HALF, HALF)
                values(NZ - 3, False, (k - 2) * HALF, HALF)

    pl.when(home)(lambda: flow(True))
    abroad(lambda: flow(False))

    state = lax.dot_general(
        weighted[...], acc[1].astype(BF16), (((0,), (0,)), ((), ())), preferred_element_type=F32
    )

    peers = [
        lax.rem(z + i, NZ) * NX + lax.rem(x + j, NX) for i in (4, 3, 5, 2, 6, 1, 7, 0) for j in (2, 1, 3, 0)
    ]

    def s_start(s, count):
        for peer in peers[:count]:
            remote(
                ssrc.at[s, peer, 0:3], sdst.at[y * NZ + z, 0:3], s_send, s_recv, {"sp": peer, "tp": up[s] * 2 + c}
            ).start()

    pl.when(home)(lambda: pl.semaphore_wait(plane_in, 1))
    abroad(lambda: pl.semaphore_wait(plane_in, 2))
    for s in (1, 0):
        part_state = state[s * CUE : (s + 1) * CUE, s * DV : (s + 1) * DV]
        term = jnp.sum(question[s * CUE : (s + 1) * CUE] * part_state, axis=0, keepdims=True)
        ssrc[s, :, 0:2] = part_state.reshape(NSP, 2, DV)
        ssrc[s, :, 2:3] = jnp.broadcast_to(term[None], (NSP, 1, DV))
        if s == 1:
            s_start(1, NSP)

    abroad(lambda: s_start(0, NSP))

    @pl.when(home)
    def _():
        s_start(0, NSP - 1)
        sdst[y * NZ + z, 0:3] = ssrc[0, sp, 0:3]

    some = sdst.at[0 : NY * NZ - 1, 0:3]
    some_sent = remote(some, some, s_send, s_recv, dev(x, y, z, 1 - c))
    whole = sdst.at[:, 0:3]
    all_sent = remote(whole, whole, s_send, s_recv, dev(x, y, z, 1 - c))
    pl.when(home)(some_sent.wait_recv)
    abroad(all_sent.wait_recv)
    total = jnp.sum(sdst[:, 0:3], axis=0)
    state_out[...] = total[0:2].astype(BF16)
    heard = total[2:3]
    square = jnp.mean(heard * heard, axis=1, keepdims=True)
    read_out[...] = (heard * lax.rsqrt(square + 1.0)).astype(BF16)

    def leave(is_home):
        slots = 1 if is_home else 2

        def left(ref, sem):
            remote(ref, ref, sem, s_recv, dev(x, y, zr)).wait_send()

        left(weight_rows(3 * HALF * slots), y_send.at[1])
        left(offs.at[0:slots], o_send)
        if is_home:
            left(weight_rows(4 * 7 * HALF), z_send)
            some_sent.wait_send()
        else:
            left(weight_rows(2 * SLICE), f_send)
            left(weight_rows(2 * 2 * (7 + 6) * HALF), z_send)
            all_sent.wait_send()

    pl.when(home)(lambda: leave(True))
    abroad(lambda: leave(False))
    ref = tok.at[0:3, 0:ROWS]
    remote(ref, ref, x_send, x_recv.at[0], dev(xr, y, z)).wait_send()
    ref = tok.at[:, 0:ROWS]
    remote(ref, ref, d_send, d_recv.at[0], dev(x, y, z, 1 - c)).wait_send()
    t1_all.wait_send()
    t2_all.wait_send()


def per_device(tokens, lock_projector, value_weight, decay_weight, decay_offset, fresh_question):
    dma = pltpu.SemaphoreType.DMA
    signal = pltpu.SemaphoreType.REGULAR
    anywhere = pl.BlockSpec(memory_space=pl.ANY)
    vmem = pl.BlockSpec(memory_space=pltpu.VMEM)
    state, read = pl.pallas_call(
        kernel,
        out_shape=(jax.ShapeDtypeStruct((2, DV), BF16), jax.ShapeDtypeStruct((1, DV), BF16)),
        in_specs=[anywhere] * 4 + [vmem] * 2,
        out_specs=(vmem, vmem),
        scratch_shapes=[
            pltpu.VMEM((NX, CHIP, D), BF16),
            pltpu.VMEM((2, D, 256), BF16),
            pltpu.VMEM((2, SLICE, 128), BF16),
            pltpu.VMEM((SLICE, 128), BF16),
            pltpu.VMEM((2 * CUE, SLICE), BF16),
            pltpu.VMEM((2 * CUE, D), BF16),
            pltpu.VMEM((2, 128), F32),
            pltpu.VMEM((2, 2, 128), F32),
            pltpu.VMEM((2, NX * CHIP, 256), F32),
            pltpu.VMEM((NX * CHIP, 128), F32),
            pltpu.VMEM((NX * CHIP, 128), BF16),
            pltpu.VMEM((NX * CHIP, 128), BF16),
            pltpu.VMEM((2, NX, 1, 128), F32),
            pltpu.VMEM((2, NY, NX, 1, 128), F32),
            pltpu.VMEM((1, 128), F32),
            pltpu.VMEM((NZ, 1, 128), F32),
            pltpu.VMEM((NX, 1, 128), F32),
            pltpu.VMEM((128, DV), F32),
            pltpu.VMEM((2, NSP, 4, DV), F32),
            pltpu.VMEM((NY * NZ, 4, DV), F32),
            dma((5,)),
            dma((2,)), dma((2, 4)),
            dma, dma,
            dma, dma,
            dma, dma((2, 4, 4)),
            dma, dma((6,)),
            dma, dma((7,)),
            dma, dma,
            dma, dma,
            dma, dma,
            signal, signal, signal,
        ],
        compiler_params=pltpu.CompilerParams(
            collective_id=0, has_side_effects=True, vmem_limit_bytes=55000 * 1024
        ),
    )(
        tokens, lock_projector.T, value_weight, decay_weight.T,
        decay_offset.reshape(1, CUE), fresh_question,
    )
    return state.reshape(1, 2, DV), read


def solution(mesh):
    in_specs = (
        P(("sp", "tp"), None),
        P(None, "tp"),
        P(None, "tp"),
        P(None, "tp"),
        P("tp"),
        P("tp", None),
    )
    out_specs = (P("tp", "sp", None), P("tp", None))
    return jax.shard_map(
        per_device, mesh=mesh, in_specs=in_specs, out_specs=out_specs, check_vma=False
    )
```

time: 201 us -> 75.7 us (0.38)
  waiting for transfers between devices: 120 us -> 0 us
  Pallas kernels: 0 us -> 72.4 us
  starting transfers between devices: 23 us -> 0 us
  other arithmetic: 22.2 us -> 0 us
  between operations: 14.9 us -> 0.66 us
  matrix products: 13.6 us -> 0 us
  local copies, waits for them, and re-layouts: 6 us -> 1.68 us
    all_gather x1 -> x0, waiting for transfers between devices: 103 us -> none  [per_device(): lax.all_gather(tokens, 'tp', axis=0, tiled=True)]
    pallas_call x0 -> x1, Pallas kernels: none -> 72.4 us  [per_device(): pl.pallas_call(kernel, out_shape=(jax.ShapeDtypeStruct((2, DV), BF16), ja...]
    all_to_all x3 -> x0, starting transfers between devices: 23 us -> none  [the longest x2 13.8 us: sent_to_all(): return lax.all_to_all(copies, axis, split_axis=0, concat_axis=0, tiled=True)]
    another operation x3 -> x0, other arithmetic: 18.5 us -> none
    all_to_all x3 -> x0, waiting for transfers between devices: 16.8 us -> none  [the longest x1 8.7 us: sent_and_summed(): lax.all_to_all(pieces, axis, split_axis=0, concat_axis=0, tiled=True)]
    dot_general x3 -> x0, matrix products: 13.6 us -> none  [the longest x1 13.1 us: per_device(): jnp.dot(lax.all_gather(tokens, 'tp', axis=0, tiled=True), combined, prefe...]
    reduce_sum x4 -> x0, other arithmetic: 2.24 us -> none  [the longest x1 1.57 us: per_device(): segment_overall = jnp.sum(log_decay, axis=0)]
  transfers between devices with their start and end apart: 4 -> 0, of which waited for: 3 -> 0; matrix products, arithmetic and copies ran while one was open for 11% -> 0% of each run, Pallas kernels for 0% -> 0%
where the time goes in v3:
time: 75.7 us; the launch traced here: 74.7 us
  Pallas kernels  72.4 us (96%)
  local copies, waits for them, and re-layouts  1.68 us (2%)
    pallas_call x1, Pallas kernels, per_device(): pl.pallas_call(kernel, out_shape=(jax.ShapeDtypeStruct((2, DV), BF16), ja...  72.4 us
    unnamed x6, local copies, waits for them, and re-layouts  1.68 us

profile of v3, /device:TPU:1, one launch (start us, length us, event | category | flops | bytes accessed | tf_op | source)
XLA Modules:
  0.0 74.7 jit_solution(3762553858885531252)
XLA Ops:
  0.6 0.0 copy-start
  0.6 0.0 copy-start.1
  0.7 0.6 copy-done
  1.3 0.0 copy-done.1
  1.3 72.4 %shard_map.77 = (bf16[2,128]{1,0:T(2,128)(2,1)S(1)}, bf16[1,128]{1,0:T(2,128)(2,1)S(1)}) custom-call(bf16[128,4096]{1,0:T(8,128)(2,1)} %tok_hbm.1, bf16[64,4096]{1,0:T(8,128)(2,1)} %bitcast.6, bf16[4096,128]{1,0:T(8,128)(2,1)} %val_hbm.1, bf16[64,4096]{1,0:T(8,128)(2,1)} %bitcast.7, f32[1,64]{1,0:T(1,128)S(1)} %bitcast.4, bf16[1,64]{1,0:T(2,128)(2,1)S(1)} %copy-done.1), custom_call_target="tpu_custom_call" | custom-call | tf_op jit(solution)/shard_map/pallas_call | solution.py:512
  73.7 0.5 copy.10
  74.2 0.5 copy.11
Async XLA Ops:
  0.6 0.7 copy-start
  0.6 0.7 copy-start.1

commit v4 on v3

--- a/solution.py
+++ b/solution.py
@@ -37,7 +37,7 @@
 def kernel(
     tok_hbm, lock_hbm, val_hbm, dec_hbm, off_ref, q_ref,
     state_out, read_out,
-    tok, w, wsrc, wfar, narrow, full, offsrc, offs, acc, after, kk, weighted,
+    tok, w, wsrc, wfar, narrow, narrow_far, full, offsrc, offs, acc, after, kk, weighted,
     tot, t1, t2src, t2, later_in_z, question, ssrc, sdst,
     load_sem, y_send, y_recv, o_send, o_recv, f_send, f_recv, z_send, z_recv, x_send, x_recv, d_send, d_recv,
     t1_send, t1_recv, t2_send, t2_recv, s_send, s_recv,
@@ -62,6 +62,19 @@
     mine = c * ROWS
     other = (1 - c) * ROWS
 
+    barrier = pltpu.get_barrier_semaphore()
+
+    def greet(device):
+        pl.semaphore_signal(barrier, inc=1, device_id=device, device_id_type=MESH)
+
+    greet(dev(x, y, z, 1 - c))
+    for i in range(1, NX):
+        greet(dev((x + i) % NX, y, z))
+    for i in range(1, NY):
+        greet(dev(x, (y + i) % NY, z))
+    greet(dev(x, y, zr))
+    greet(dev(x, y, zl))
+
     zrow = pl.multiple_of(z * SLICE, SLICE)
     zfar = pl.multiple_of((z + 4) % NZ * SLICE, SLICE)
     loads = [
@@ -69,7 +82,9 @@
         pltpu.make_async_copy(dec_hbm.at[:, pl.ds(zrow, SLICE)], narrow.at[CUE : 2 * CUE], load_sem.at[0]),
         pltpu.make_async_copy(val_hbm.at[pl.ds(zrow, SLICE)], wsrc.at[1], load_sem.at[1]),
         pltpu.make_async_copy(tok_hbm, tok.at[0, pl.ds(pl.multiple_of(mine, ROWS), ROWS)], load_sem.at[2]),
-        pltpu.make_async_copy(val_hbm.at[pl.ds(zfar, SLICE)], wfar, load_sem.at[3]),
+        pltpu.make_async_copy(val_hbm.at[pl.ds(zfar, SLICE)], wfar.at[1], load_sem.at[3]),
+        pltpu.make_async_copy(lock_hbm.at[:, pl.ds(zfar, SLICE)], narrow_far.at[0:CUE], load_sem.at[5]),
+        pltpu.make_async_copy(dec_hbm.at[:, pl.ds(zfar, SLICE)], narrow_far.at[CUE : 2 * CUE], load_sem.at[5]),
     ]
     for load in loads:
         load.start()
@@ -85,19 +100,6 @@
         for load in own_loads:
             load.start()
 
-    barrier = pltpu.get_barrier_semaphore()
-
-    def greet(device):
-        pl.semaphore_signal(barrier, inc=1, device_id=device, device_id_type=MESH)
-
-    greet(dev(x, y, z, 1 - c))
-    for i in range(1, NX):
-        greet(dev((x + i) % NX, y, z))
-    for i in range(1, NY):
-        greet(dev(x, (y + i) % NY, z))
-    greet(dev(x, y, zr))
-    greet(dev(x, y, zl))
-
     def t1_peer(s, dy):
         yy = (y + dy) % NY
         d = (up[s] - yy + NY) % NY
@@ -138,17 +140,22 @@
     def o_copy(s):
         return remote(offsrc, offs.at[s], o_send, o_recv, dev(x, down[s], z))
 
-    def far_copy(s):
+    def far_copy(s, t):
         return remote(
-            wfar, w.at[1, pl.ds(zfar, SLICE), pl.ds(s * 128, 128)],
-            f_send, f_recv, dev(x, down[s], z),
+            wfar.at[t], w.at[t, pl.ds(zfar, SLICE), pl.ds(s * 128, 128)],
+            f_send, f_recv.at[t], dev(x, down[s], z),
         )
 
     def abroad(action):
         pl.when(jnp.logical_not(home))(action)
 
     y_copy(1, 0).start()
-    abroad(lambda: y_copy(0, 0).start())
+
+    @abroad
+    def _():
+        y_copy(0, 0).start()
+        y_copy(0, 1).start()
+
 
     def x_rows(direction, p):
         half = direction if p in (0, 1, 4, 5) else 1 - direction
@@ -313,42 +320,58 @@
             for s in slots:
                 y_copy(s, k).start()
 
-        def own(k):
-            for s in slots:
+        def own(k, only=slots):
+            for s in only:
                 y_copy(s, k).wait_recv()
                 for direction in range(2):
                     z_copy(s, direction, k, 0).start()
 
-        def hop(k, d):
-            for s in slots:
+        def hop(k, d, only=slots):
+            for s in only:
                 z_wait(s, k, d - 1)
                 for direction in range(2):
                     z_copy(s, direction, k, d).start()
 
         def last(k):
-            for s in slots:
-                z_wait(s, k, 3)
+            z_wait(1, k, 3)
 
         ref = weight_rows(HALF * len(slots))
         remote(ref, ref, y_send.at[0], y_recv.at[1, 0], dev(x, y, zr)).wait_send()
-        y_start(1)
+        y_copy(1, 1).start()
         for s in slots:
             o_copy(s).start()
         loads[4].wait()
+        pltpu.make_async_copy(narrow_far, narrow_far, load_sem.at[5]).wait()
         if is_home:
             pltpu.make_async_copy(w.at[0], w.at[0], load_sem.at[4]).wait()
             for i in range(NZ):
                 w[0, i * SLICE : (i + 1) * SLICE, 0:128] = full[:, i * SLICE : (i + 1) * SLICE].T
             offs[0] = offsrc[...]
-        own(0)
         if is_home:
+            own(0)
             y_start(2)
             y_start(3)
-        own(1)
-        if not is_home:
+            own(1)
+            hop(0, 1)
+        else:
+            wfar[0] = narrow_far[...].T
+            own(0, (0,))
+
+            @pl.when(x == 2)
+            def _():
+                own(0, (1,))
+                own(1, (0,))
+
+            @pl.when(x != 2)
+            def _():
+                own(1, (0,))
+                own(0, (1,))
+
+            far_copy(0, 0).start()
+            hop(0, 1)
+            own(1, (1,))
             y_start(2)
             y_start(3)
-        hop(0, 1)
         hop(1, 1)
         hop(0, 2)
         pieces_in(0)
@@ -356,10 +379,14 @@
         hop(1, 2)
         if not is_home:
             for s in slots:
-                far_copy(s).start()
-        hop(0, 3)
+                far_copy(s, 1).start()
+        if not is_home:
+            z_wait(0, 0, 2)
+        hop(0, 3, (1,))
         own(2)
-        hop(1, 3)
+        if not is_home:
+            z_wait(0, 1, 2)
+        hop(1, 3, (1,))
         own(3)
         offs_in = offs.at[0 : len(slots)]
         remote(offs_in, offs_in, o_send, o_recv, dev(x, y, zr)).wait_recv()
@@ -375,6 +402,9 @@
         last(0)
         hop(2, 1)
         last(1)
+        if not is_home:
+            ref = weight_rows(SLICE)
+            remote(ref, ref, f_send, f_recv.at[0], dev(x, y, zr)).wait_recv()
         for i in range(1, NX):
             tell(column_in, dev((x + i) % NX, y, z))
         keys(3)
@@ -422,7 +452,7 @@
             values(4)
         else:
             ref = weight_rows(2 * SLICE)
-            remote(ref, ref, f_send, f_recv, dev(x, y, zr)).wait_recv()
+            remote(ref, ref, f_send, f_recv.at[1], dev(x, y, zr)).wait_recv()
             values(4)
             for k in (2, 3):
                 if k == 3:
@@ -490,8 +520,8 @@
             left(weight_rows(4 * 7 * HALF), z_send)
             some_sent.wait_send()
         else:
-            left(weight_rows(2 * SLICE), f_send)
-            left(weight_rows(2 * 2 * (7 + 6) * HALF), z_send)
+            left(weight_rows(3 * SLICE), f_send)
+            left(weight_rows(2 * (12 + 13) * HALF), z_send)
             all_sent.wait_send()
 
     pl.when(home)(lambda: leave(True))
@@ -518,7 +548,8 @@
             pltpu.VMEM((NX, CHIP, D), BF16),
             pltpu.VMEM((2, D, 256), BF16),
             pltpu.VMEM((2, SLICE, 128), BF16),
-            pltpu.VMEM((SLICE, 128), BF16),
+            pltpu.VMEM((2, SLICE, 128), BF16),
+            pltpu.VMEM((2 * CUE, SLICE), BF16),
             pltpu.VMEM((2 * CUE, SLICE), BF16),
             pltpu.VMEM((2 * CUE, D), BF16),
             pltpu.VMEM((2, 128), F32),
@@ -535,10 +566,10 @@
             pltpu.VMEM((128, DV), F32),
             pltpu.VMEM((2, NSP, 4, DV), F32),
             pltpu.VMEM((NY * NZ, 4, DV), F32),
-            dma((5,)),
+            dma((6,)),
             dma((2,)), dma((2, 4)),
             dma, dma,
-            dma, dma,
+            dma, dma((2,)),
             dma, dma((2, 4, 4)),
             dma, dma((6,)),
             dma, dma((7,)),

time: 75.7 us -> 74 us (0.978); the launches traced: 74.7 us -> 73.8 us
  Pallas kernels: 72.4 us -> 71.5 us
    pallas_call x1, Pallas kernels: 72.4 us -> 71.5 us  [per_device(): pl.pallas_call(kernel, out_shape=(jax.ShapeDtypeStruct((2, DV), BF16), ja...]
where the time goes in v4:
time: 74 us; the launch traced here: 73.8 us
  Pallas kernels  71.5 us (97%)
  local copies, waits for them, and re-layouts  1.68 us (2%)
    pallas_call x1, Pallas kernels, per_device(): pl.pallas_call(kernel, out_shape=(jax.ShapeDtypeStruct((2, DV), BF16), ja...  71.5 us
    unnamed x6, local copies, waits for them, and re-layouts  1.68 us

profile of v4, /device:TPU:1, one launch (start us, length us, event | category | flops | bytes accessed | tf_op | source)
XLA Modules:
  0.0 73.8 jit_solution(1227033801469975936)
XLA Ops:
  0.6 0.0 copy-start
  0.6 0.0 copy-start.1
  0.7 0.6 copy-done
  1.3 0.0 copy-done.1
  1.3 71.5 %shard_map.77 = (bf16[2,128]{1,0:T(2,128)(2,1)S(1)}, bf16[1,128]{1,0:T(2,128)(2,1)S(1)}) custom-call(bf16[128,4096]{1,0:T(8,128)(2,1)} %tok_hbm.1, bf16[64,4096]{1,0:T(8,128)(2,1)} %bitcast.6, bf16[4096,128]{1,0:T(8,128)(2,1)} %val_hbm.1, bf16[64,4096]{1,0:T(8,128)(2,1)} %bitcast.7, f32[1,64]{1,0:T(1,128)S(1)} %bitcast.4, bf16[1,64]{1,0:T(2,128)(2,1)S(1)} %copy-done.1), custom_call_target="tpu_custom_call" | custom-call | tf_op jit(solution)/shard_map/pallas_call | solution.py:542
  72.8 0.5 copy.10
  73.3 0.5 copy.11
Async XLA Ops:
  0.6 0.7 copy-start
  0.6 0.7 copy-start.1

commit v5 on v4

--- a/solution.py
+++ b/solution.py
@@ -412,11 +412,11 @@
         keys(4)
         hop(3, 1)
         pieces_in(4)
+        decay(0)
+        decay(1)
         pieces_in(5)
         if is_home:
             hop(2, 2)
-        decay(0)
-        decay(1)
         decay(2)
         if is_home:
             hop(3, 2)
@@ -446,21 +446,20 @@
         if is_home:
             values(3)
             values(NZ - 3)
-            t2_end()
             for k in (2, 3):
                 z_wait(1, k, 3)
             values(4)
+            t2_end()
         else:
             ref = weight_rows(2 * SLICE)
             remote(ref, ref, f_send, f_recv.at[1], dev(x, y, zr)).wait_recv()
             values(4)
             for k in (2, 3):
-                if k == 3:
-                    t2_end()
                 for s in slots:
                     z_wait(s, k, 2)
                 values(3, False, (k - 2) * HALF, HALF)
                 values(NZ - 3, False, (k - 2) * HALF, HALF)
+            t2_end()
 
     pl.when(home)(lambda: flow(True))
     abroad(lambda: flow(False))

time: 74 us -> 73.3 us (level)
  no operation moved by 1% of the time
where the time goes in v5:
time: 73.3 us; the launch traced here: 73.1 us
  Pallas kernels  70.8 us (97%)
  local copies, waits for them, and re-layouts  1.68 us (2%)
    pallas_call x1, Pallas kernels, per_device(): pl.pallas_call(kernel, out_shape=(jax.ShapeDtypeStruct((2, DV), BF16), ja...  70.8 us
    unnamed x6, local copies, waits for them, and re-layouts  1.68 us

profile of v5, /device:TPU:1, one launch (start us, length us, event | category | flops | bytes accessed | tf_op | source)
XLA Modules:
  0.0 73.1 jit_solution(927910515381952723)
XLA Ops:
  0.6 0.0 copy-start
  0.6 0.0 copy-start.1
  0.7 0.6 copy-done
  1.3 0.0 copy-done.1
  1.3 70.8 %shard_map.77 = (bf16[2,128]{1,0:T(2,128)(2,1)S(1)}, bf16[1,128]{1,0:T(2,128)(2,1)S(1)}) custom-call(bf16[128,4096]{1,0:T(8,128)(2,1)} %tok_hbm.1, bf16[64,4096]{1,0:T(8,128)(2,1)} %bitcast.6, bf16[4096,128]{1,0:T(8,128)(2,1)} %val_hbm.1, bf16[64,4096]{1,0:T(8,128)(2,1)} %bitcast.7, f32[1,64]{1,0:T(1,128)S(1)} %bitcast.4, bf16[1,64]{1,0:T(2,128)(2,1)S(1)} %copy-done.1), custom_call_target="tpu_custom_call" | custom-call | tf_op jit(solution)/shard_map/pallas_call | solution.py:541
  72.1 0.5 copy.10
  72.6 0.5 copy.11
Async XLA Ops:
  0.6 0.7 copy-start
  0.6 0.7 copy-start.1

commit v6 on v5

--- a/solution.py
+++ b/solution.py
@@ -37,7 +37,7 @@
 def kernel(
     tok_hbm, lock_hbm, val_hbm, dec_hbm, off_ref, q_ref,
     state_out, read_out,
-    tok, w, wsrc, wfar, narrow, narrow_far, full, offsrc, offs, acc, after, kk, weighted,
+    tok, w, wsrc, wfar, narrow, narrow_far, full, offsrc, offs, acc, projected, after, kk, weighted,
     tot, t1, t2src, t2, later_in_z, question, ssrc, sdst,
     load_sem, y_send, y_recv, o_send, o_recv, f_send, f_recv, z_send, z_recv, x_send, x_recv, d_send, d_recv,
     t1_send, t1_recv, t2_send, t2_recv, s_send, s_recv,
@@ -283,6 +283,12 @@
     t2_all = remote(t2_bytes, t2_bytes, t2_send, t2_recv, dev(x, y, z, 1 - c))
 
     def t1_end():
+        eye = (
+            lax.broadcasted_iota(jnp.int32, (128, 128), 0) == lax.broadcasted_iota(jnp.int32, (128, 128), 1)
+        )
+        asked = jnp.where(low, offs[0, 1:2], offs[1, 1:2]) * CUE ** -0.5
+        column = jnp.sum(jnp.where(eye, asked, 0.0), axis=1, keepdims=True)
+        question[...] = jnp.broadcast_to(column, question.shape)
         t1_all.wait_recv()
         blocks = jnp.where(low[None, None], t1[0], t1[1])
         per_x = jnp.sum(blocks, axis=0)
@@ -298,6 +304,7 @@
             later = later + per_x[b]
 
     def t2_end():
+        projected[...] = acc[1].astype(BF16)
         t2_all.wait_recv()
         spans = t2[...]
         z_index = lax.broadcasted_iota(jnp.int32, spans.shape, 0)
@@ -306,12 +313,6 @@
             rows = pl.ds(b * CHIP, CHIP)
             factor = jnp.exp(after[rows] + (later + later_in_z[place[b]]))
             weighted[rows] = (kk[rows].astype(F32) * factor).astype(BF16)
-        eye = (
-            lax.broadcasted_iota(jnp.int32, (128, 128), 0) == lax.broadcasted_iota(jnp.int32, (128, 128), 1)
-        )
-        asked = jnp.where(low, offs[0, 1:2], offs[1, 1:2]) * CUE ** -0.5
-        column = jnp.sum(jnp.where(eye, asked, 0.0), axis=1, keepdims=True)
-        question[...] = jnp.broadcast_to(column, question.shape)
 
     def flow(is_home):
         slots = (1,) if is_home else (0, 1)
@@ -465,7 +466,7 @@
     abroad(lambda: flow(False))
 
     state = lax.dot_general(
-        weighted[...], acc[1].astype(BF16), (((0,), (0,)), ((), ())), preferred_element_type=F32
+        weighted[...], projected[...], (((0,), (0,)), ((), ())), preferred_element_type=F32
     )
 
     peers = [
@@ -554,6 +555,7 @@
             pltpu.VMEM((2, 128), F32),
             pltpu.VMEM((2, 2, 128), F32),
             pltpu.VMEM((2, NX * CHIP, 256), F32),
+            pltpu.VMEM((NX * CHIP, 256), BF16),
             pltpu.VMEM((NX * CHIP, 128), F32),
             pltpu.VMEM((NX * CHIP, 128), BF16),
             pltpu.VMEM((NX * CHIP, 128), BF16),

time: 73.3 us -> 73.2 us (level)
  no operation moved by 1% of the time
where the time goes in v6:
time: 73.2 us; the launch traced here: 73 us
  Pallas kernels  70.7 us (97%)
  local copies, waits for them, and re-layouts  1.68 us (2%)
    pallas_call x1, Pallas kernels, per_device(): pl.pallas_call(kernel, out_shape=(jax.ShapeDtypeStruct((2, DV), BF16), ja...  70.7 us
    unnamed x6, local copies, waits for them, and re-layouts  1.68 us

profile of v6, /device:TPU:1, one launch (start us, length us, event | category | flops | bytes accessed | tf_op | source)
XLA Modules:
  0.0 73.0 jit_solution(3056449153597742786)
XLA Ops:
  0.6 0.0 copy-start
  0.6 0.0 copy-start.1
  0.7 0.6 copy-done
  1.3 0.0 copy-done.1
  1.3 70.7 %shard_map.77 = (bf16[2,128]{1,0:T(2,128)(2,1)S(1)}, bf16[1,128]{1,0:T(2,128)(2,1)S(1)}) custom-call(bf16[128,4096]{1,0:T(8,128)(2,1)} %tok_hbm.1, bf16[64,4096]{1,0:T(8,128)(2,1)} %bitcast.6, bf16[4096,128]{1,0:T(8,128)(2,1)} %val_hbm.1, bf16[64,4096]{1,0:T(8,128)(2,1)} %bitcast.7, f32[1,64]{1,0:T(1,128)S(1)} %bitcast.4, bf16[1,64]{1,0:T(2,128)(2,1)S(1)} %copy-done.1), custom_call_target="tpu_custom_call" | custom-call | tf_op jit(solution)/shard_map/pallas_call | solution.py:542
  72.0 0.5 copy.10
  72.5 0.5 copy.11
Async XLA Ops:
  0.6 0.7 copy-start
  0.6 0.7 copy-start.1
